TPU v7x, 32 devices: a whole 2x2x4 slice. The times are simulated.
32 devices in a mesh: sp: 4 (over y, x), tp: 8 (over z, core).
Axes of the slice: x: 2, y: 2, z: 4, core: 2. Of those that a mesh axis runs over, the one named last changes fastest.
Arguments:
- conv_value: bfloat16 [6144, 2048], P('sp', 'tp'), may hold values from -48 to 48
- conv_gate: bfloat16 [6144, 2048], P('sp', 'tp'), may hold values from -6 to 6
- doc_ids: int32 [6144], P('sp'), may hold values from 0 to 3, never falling along the last dimension, each value on 1 to 4608 neighbouring positions
- conv_kernel: bfloat16 [31, 2048], P(None, 'tp'), may hold values from -1 to 1
- norm_gain_conv: float32 [2048], replicated, may hold values from 0.1 to 1.9
- norm_bias_conv: float32 [2048], replicated, may hold values from -3 to 3
- proj_weight: bfloat16 [2048, 2048], P('tp'), may hold values from -0.125 to 0.125
- residual: bfloat16 [6144, 2048], P(('sp', 'tp')), may hold values from -6 to 6
- norm_gain_moe: float32 [2048], replicated, may hold values from 0.1 to 1.9
- group_router: bfloat16 [2048, 2], replicated, may hold values from -0.125 to 0.125
- expert_router: bfloat16 [2048, 4], replicated, may hold values from -0.125 to 0.125
- routing: int32 [6144, 2], P(('sp', 'tp')), may hold values from 0 to 3, as said below
- expert_gate_w: bfloat16 [4, 2048, 512], P('sp'), may hold values from -0.125 to 0.125
- expert_up_w: bfloat16 [4, 2048, 512], P('sp'), may hold values from -0.125 to 0.125
- expert_down_w: bfloat16 [4, 512, 2048], P('sp'), may hold values from -0.25 to 0.25
Outputs:
- output: bfloat16 [6144, 2048], P(('sp', 'tp'))
Inputs may be any that keep to these rules, and one draw needn't show every extreme that they name: `routing`: both numbers of a row are different experts of one group (expert // 2); within the rows of one device (aligned blocks of 192 rows) every expert is named exactly 96 times.
All inputs are finite; a program needn't handle non-finite values.
Results may differ from a plain program's by a relative error of at most 0.015.
Values may be sent and summed in bfloat16 or wider, within the bound.
A program may use at most 64 MiB of HBM per device.

v0:
```python
import functools

import jax
import jax.numpy as jnp
from jax import lax
from jax.experimental import pallas as pl
from jax.experimental.pallas import tpu as pltpu
from jax.sharding import PartitionSpec as P

epsilon = 1e-06
MESH = pl.DeviceIdType.MESH
F32 = jnp.float32
BF16 = jnp.bfloat16
HALO = 32


def gate(value, gate_value):
    return (value.astype(F32) * jax.nn.sigmoid(gate_value.astype(F32))).astype(BF16)


def kernel(
    S,
    T,
    G,
    value_hbm,
    gate_hbm,
    least_tap_ref,
    ids_ref,
    kernel_ref,
    gain_conv_ref,
    bias_conv_ref,
    weight_hbm,
    residual_hbm,
    gain_moe_ref,
    group_router_ref,
    expert_router_ref,
    routing_ref,
    gate_w_hbm,
    up_w_hbm,
    down_w_hbm,
    out_ref,
    value,
    gates,
    wfull,
    residual,
    gate_w,
    up_w,
    down_w,
    rim_out,
    rim_in,
    padded,
    taps,
    conv_out,
    conv_in,
    act,
    hidden,
    normed,
    outgoing,
    arrived,
    ffn_hidden,
    results,
    returned,
    local_sem,
    wl_sem,
    rim_sem,
    wz_send,
    wz_recv,
    wx_send,
    wx_recv,
    wp_send,
    wp_recv,
    a2a_send,
    a2a_recv,
    disp_send,
    disp_recv,
    ret_send,
    ret_recv,
):
    s = lax.axis_index("sp")
    t = lax.axis_index("tp")
    Z = T // 2
    z = t // 2
    core = t % 2
    partner = 2 * z + 1 - core
    tokens, width = value.shape
    block = tokens // T
    n_taps = kernel_ref.shape[0]
    piece = wfull.shape[3]
    D = S * piece

    def remote(src, dst, send, recv, sp_to, tp_to):
        return pltpu.make_async_remote_copy(
            src_ref=src,
            dst_ref=dst,
            send_sem=send,
            recv_sem=recv,
            device_id=(sp_to, tp_to),
            device_id_type=MESH,
        )

    loads = [
        pltpu.make_async_copy(a, b, local_sem.at[i])
        for i, (a, b) in enumerate(
            [
                (value_hbm, value),
                (gate_hbm, gates),
                (residual_hbm, residual),
                (gate_w_hbm, gate_w),
                (up_w_hbm, up_w),
                (down_w_hbm, down_w),
            ]
        )
    ]
    own_w = [
        pltpu.make_async_copy(
            weight_hbm.at[:, pl.ds(j * piece, piece)], wfull.at[t, j], wl_sem.at[j]
        )
        for j in range(S)
    ]
    loads[0].start()
    loads[1].start()
    for c in own_w:
        c.start()
    for c in loads[2:]:
        c.start()

    barrier = pltpu.get_barrier_semaphore()
    for k in range(1, T):
        pl.semaphore_signal(
            barrier, inc=1, device_id=(s, lax.rem(t + k, T)), device_id_type=MESH
        )
    for k in range(1, S):
        pl.semaphore_signal(
            barrier, inc=1, device_id=(lax.rem(s + k, S), t), device_id_type=MESH
        )
    pl.semaphore_wait(barrier, T + S - 2)

    for c in own_w:
        c.wait()
    waits = []
    for k in range(1, Z):
        to = 2 * lax.rem(z + k, Z) + core
        c = remote(wfull.at[t, s], wfull.at[t, s], wz_send.at[k], wz_recv.at[z], s, to)
        c.start()
        waits.append(c)
    c = remote(wfull.at[t], wfull.at[t], wp_send.at[z], wp_recv.at[z], s, partner)
    c.start()
    waits.append(c)

    loads[0].wait()
    loads[1].wait()
    tail = pl.ds(tokens - HALO, HALO)
    last_reach = jnp.max(least_tap_ref[tokens - 1 : tokens, :], axis=1, keepdims=True)
    newer = lax.broadcasted_iota(jnp.int32, (HALO, width), 0) >= last_reach + HALO - n_taps
    rim = jnp.where(newer, gate(value[tail, :], gates[tail, :]).astype(F32), jnp.float32(0.0))
    rim_out[0:HALO, :] = rim.astype(BF16)
    rim_out[HALO : HALO + 16, :] = jnp.full(
        (16, width), ids_ref[tokens - 1].astype(F32), F32
    ).astype(BF16)
    rim_copy = remote(
        rim_out, rim_in, rim_sem.at[0], rim_sem.at[1], lax.rem(s + 1, S), t
    )
    rim_copy.start()

    def gate_rows(i, _):
        rows = pl.ds(pl.multiple_of(i * 64, 64), 64)
        to_rows = pl.ds(pl.multiple_of(HALO + i * 64, 32), 64)
        padded[to_rows, :] = gate(value[rows, :], gates[rows, :]).astype(F32)
        return 0

    lax.fori_loop(0, tokens // 64, gate_rows, 0)
    taps[0:n_taps, :] = kernel_ref[...].astype(F32)
    rim_copy.wait()
    same = (rim_in[HALO : HALO + 1, :].astype(F32) == ids_ref[0].astype(F32)) & (s > 0)
    padded[0:HALO, :] = jnp.where(same, rim_in[0:HALO, :].astype(F32), jnp.float32(0.0))

    step_rows = 32 if block % 32 == 0 else 8
    lanes = min(width, 128)

    def conv_block(owner):
        def conv_rows(i, _):
            base = pl.multiple_of(owner * block + i * step_rows, 8)
            least = least_tap_ref[pl.ds(base, step_rows), :]
            window = padded[pl.ds(base, step_rows + HALO), :]
            total = jnp.zeros((step_rows, width), F32)
            for tap in range(n_taps):
                at = tap + HALO + 1 - n_taps
                valid = least <= tap
                product = window[at : at + step_rows, :] * taps[tap : tap + 1, :]
                parts = [
                    jnp.where(valid, product[:, j : j + lanes], jnp.float32(0.0))
                    for j in range(0, width, lanes)
                ]
                total = total + jnp.concatenate(parts, axis=1)
            conv_out[
                owner, pl.ds(pl.multiple_of(i * step_rows, step_rows), step_rows), :
            ] = total.astype(BF16)
            return 0

        lax.fori_loop(0, block // step_rows, conv_rows, 0)

    def conv_send(k, _):
        owner = lax.rem(t + k, T)
        conv_block(owner)
        remote(
            conv_out.at[owner],
            conv_in.at[t],
            a2a_send.at[owner],
            a2a_recv.at[t],
            s,
            owner,
        ).start()
        return 0

    done = 1
    for k in range(1, Z):
        upto = T - 2 * (Z - 1 - k)
        lax.fori_loop(done, upto, conv_send, 0)
        done = upto
        from_z = lax.rem(z - k + Z, Z)
        row = 2 * from_z + core
        remote(
            wfull.at[row, s], wfull.at[row, s], wz_send.at[k], wz_recv.at[from_z], s, t
        ).wait_recv()
        for j in range(1, S):
            c = remote(
                wfull.at[row, s],
                wfull.at[row, s],
                wx_send.at[j, from_z],
                wx_recv.at[s, from_z],
                lax.rem(s + j, S),
                t,
            )
            c.start()
            waits.append(c)
    conv_block(t)
    conv_in[t, :, :] = conv_out[t, :, :]

    rows = block
    E = S
    cap = 2 * rows // E
    lane = lax.broadcasted_iota(jnp.int32, (rows, 128), 1)
    eye = lax.broadcasted_iota(jnp.int32, (rows, rows), 0) == lax.broadcasted_iota(
        jnp.int32, (rows, rows), 1
    )
    named = lax.dot_general(
        eye.astype(F32).astype(BF16),
        routing_ref[...].astype(F32).astype(BF16),
        (((1,), (1,)), ((), ())),
        preferred_element_type=F32,
    )
    first = named[:, 0:1]
    second = named[:, 1:2]
    lane_f = lane.astype(F32)
    chosen = (lane_f == first) | (lane_f == second)
    per_group = E // G
    group_low = lane_f * per_group
    in_group = (first >= group_low) & (first < group_low + per_group)
    tri = lax.broadcasted_iota(jnp.int32, (rows, rows), 0) > lax.broadcasted_iota(
        jnp.int32, (rows, rows), 1
    )
    before = jnp.dot(
        tri.astype(F32).astype(BF16),
        chosen.astype(F32).astype(BF16),
        preferred_element_type=F32,
    )
    slot = jnp.where(chosen, before, jnp.float32(-1.0))

    for k in range(1, T):
        source = lax.rem(t + k, T)
        remote(
            conv_out.at[source], conv_in.at[source], a2a_send.at[source], a2a_recv.at[source], s, source
        ).wait_recv()
    total = jnp.zeros((rows, 1), F32)
    for j in range(T):
        total = total + jnp.sum(conv_in[j].astype(F32), axis=1, keepdims=True)
    average = total / (T * width)
    total = jnp.zeros((rows, 1), F32)
    for j in range(T):
        centered = conv_in[j].astype(F32) - average
        total = total + jnp.sum(centered * centered, axis=1, keepdims=True)
    scale = lax.rsqrt(total / (T * width) + epsilon)
    for j in range(T):
        cols = slice(j * width, (j + 1) * width)
        v = (conv_in[j].astype(F32) - average) * scale * gain_conv_ref[:, cols] + bias_conv_ref[
            :, cols
        ]
        act[j, :, :] = (v / (1.0 + jnp.exp(-v))).astype(BF16)

    for k in range(1, Z):
        from_z = lax.rem(z - k + Z, Z)
        row = 2 * from_z + core
        for j in range(1, S):
            source = lax.rem(s - j + S, S)
            remote(
                wfull.at[row, source],
                wfull.at[row, source],
                wx_send.at[j, from_z],
                wx_recv.at[source, from_z],
                source,
                t,
            ).wait_recv()
        c = remote(
            wfull.at[row], wfull.at[row], wp_send.at[from_z], wp_recv.at[from_z], s, partner
        )
        c.start()
        waits.append(c)
    loads[2].wait()
    for j in range(Z):
        row = 2 * j + 1 - core
        remote(wfull.at[row], wfull.at[row], wp_send.at[j], wp_recv.at[j], s, partner).wait_recv()

    def project(j, squares):
        cols = pl.ds(pl.multiple_of(j * piece, piece), piece)
        acc = residual[:, cols].astype(F32)
        part = jnp.zeros_like(acc)
        for i in range(T):
            part = part + jnp.dot(act[i], wfull[i, j], preferred_element_type=F32)
        state = (acc + part).astype(BF16)
        hidden[:, cols] = state
        state = state.astype(F32)
        return squares + jnp.sum(state * state, axis=1, keepdims=True)

    squares = lax.fori_loop(0, S, project, jnp.zeros((rows, 1), F32))
    scale = lax.rsqrt(squares / D + epsilon)

    def norm_cols(j, _):
        cols = pl.ds(pl.multiple_of(j * piece, piece), piece)
        normed[:, cols] = (hidden[:, cols].astype(F32) * scale * gain_moe_ref[:, cols]).astype(BF16)
        return 0

    lax.fori_loop(0, S, norm_cols, 0)

    slot_iota = lax.broadcasted_iota(jnp.int32, (rows, cap), 1).astype(F32)

    def column(array, expert):
        mine = lane[:, : array.shape[1]] == expert
        return jnp.sum(jnp.where(mine, array, jnp.float32(0.0)), axis=1, keepdims=True)

    def gather_rows(expert, target):
        picks = (column(slot, expert) == slot_iota).astype(F32).astype(BF16)

        def cols_step(j, _):
            cols = pl.ds(pl.multiple_of(j * piece, piece), piece)
            target[:, cols] = lax.dot_general(
                picks,
                normed[:, cols],
                (((0,), (0,)), ((), ())),
                preferred_element_type=F32,
            ).astype(BF16)
            return 0

        lax.fori_loop(0, S, cols_step, 0)

    for k in range(1, S):
        expert = lax.rem(s + k, S)
        gather_rows(expert, outgoing.at[expert])
        remote(
            outgoing.at[expert], arrived.at[s], disp_send.at[expert], disp_recv.at[s], expert, t
        ).start()
    gather_rows(s, arrived.at[s])

    def logits(router):
        return lax.dot_general(
            normed[...], router[...], (((1,), (1,)), ((), ())), preferred_element_type=F32
        )

    group_exp = jnp.exp(logits(group_router_ref))
    expert_exp = jnp.exp(logits(expert_router_ref))
    zero = jnp.float32(0.0)
    group_prob = jnp.sum(
        jnp.where(in_group[:, :G], group_exp, zero), axis=1, keepdims=True
    ) / jnp.sum(group_exp, axis=1, keepdims=True)
    chosen_exp = jnp.where(chosen[:, :E], expert_exp, zero)
    mix = group_prob * chosen_exp / jnp.sum(chosen_exp, axis=1, keepdims=True)

    for c in loads[3:]:
        c.wait()
    ff = gate_w.shape[2]
    ff_step = min(ff, 256)

    def expert_block(sender, target):
        def up_step(j, _):
            cols = pl.ds(pl.multiple_of(j * ff_step, ff_step), ff_step)
            x = arrived[sender]
            g = jnp.dot(x, gate_w[0, :, cols], preferred_element_type=F32)
            u = jnp.dot(x, up_w[0, :, cols], preferred_element_type=F32)
            ffn_hidden[:, cols] = (g / (1.0 + jnp.exp(-g)) * u).astype(BF16)
            return 0

        lax.fori_loop(0, ff // ff_step, up_step, 0)

        def down_step(j, _):
            cols = pl.ds(pl.multiple_of(j * piece, piece), piece)
            target[:, cols] = jnp.dot(
                ffn_hidden[...], down_w[0, :, cols], preferred_element_type=F32
            ).astype(BF16)
            return 0

        lax.fori_loop(0, S, down_step, 0)

    expert_block(s, returned.at[s])
    for k in range(1, S):
        sender = lax.rem(s - k + S, S)
        remote(
            outgoing.at[sender], arrived.at[sender], disp_send.at[sender], disp_recv.at[sender], sender, t
        ).wait_recv()
        expert_block(sender, results.at[sender])
        remote(
            results.at[sender], returned.at[s], ret_send.at[sender], ret_recv.at[s], sender, t
        ).start()

    for k in range(1, S):
        expert = lax.rem(s + k, S)
        remote(
            results.at[expert], returned.at[expert], ret_send.at[expert], ret_recv.at[expert], expert, t
        ).wait_recv()
    spreads = [
        jnp.where(column(slot, e) == slot_iota, column(mix, e), zero).astype(BF16)
        for e in range(E)
    ]

    def combine(j, _):
        cols = pl.ds(pl.multiple_of(j * piece, piece), piece)
        acc = jnp.zeros((rows, piece), F32)
        for e in range(E):
            acc = acc + jnp.dot(spreads[e], returned[e, :, cols], preferred_element_type=F32)
        out_ref[:, cols] = (hidden[:, cols].astype(F32) + acc).astype(BF16)
        return 0

    lax.fori_loop(0, S, combine, 0)

    for c in waits:
        c.wait_send()
    for k in range(1, T):
        to = lax.rem(t + k, T)
        remote(conv_out.at[to], conv_in.at[t], a2a_send.at[to], a2a_recv.at[t], s, to).wait_send()
    for k in range(1, S):
        to = lax.rem(s + k, S)
        remote(outgoing.at[to], arrived.at[s], disp_send.at[to], disp_recv.at[s], to, t).wait_send()
        remote(results.at[to], returned.at[s], ret_send.at[to], ret_recv.at[s], to, t).wait_send()


def body(
    S,
    T,
    conv_value,
    conv_gate,
    doc_ids,
    conv_kernel,
    norm_gain_conv,
    norm_bias_conv,
    proj_weight,
    residual,
    norm_gain_moe,
    group_router,
    expert_router,
    routing,
    expert_gate_w,
    expert_up_w,
    expert_down_w,
):
    tokens, width = conv_value.shape
    n_taps = conv_kernel.shape[0]
    rows, D = residual.shape
    wrows = proj_weight.shape[0]
    ff = expert_gate_w.shape[2]
    G = group_router.shape[1]
    E = expert_router.shape[1]
    cap = 2 * rows // E
    lanes = min(width, 128)
    start = jnp.sum((doc_ids[None, :] < doc_ids[:, None]).astype(jnp.int32), axis=1)
    position = jnp.arange(tokens, dtype=jnp.int32)
    least = jnp.where(start == 0, 0, n_taps - 1 - (position - start))
    least_tap = jnp.broadcast_to(least[:, None], (tokens, lanes))
    vmem = pl.BlockSpec(memory_space=pltpu.VMEM)
    hbm = pl.BlockSpec(memory_space=pl.ANY)
    smem = pl.BlockSpec(memory_space=pltpu.SMEM)
    dma = pltpu.SemaphoreType.DMA
    piece = D // S
    Z = T // 2
    return pl.pallas_call(
        functools.partial(kernel, S, T, G),
        out_shape=jax.ShapeDtypeStruct((rows, D), BF16),
        in_specs=[
            hbm, hbm, vmem, smem, vmem, vmem, vmem, hbm, hbm, vmem, vmem, vmem, vmem,
            hbm, hbm, hbm,
        ],
        out_specs=vmem,
        scratch_shapes=[
            pltpu.VMEM((tokens, width), BF16),
            pltpu.VMEM((tokens, width), BF16),
            pltpu.VMEM((T, S, wrows, piece), BF16),
            pltpu.VMEM((rows, D), BF16),
            pltpu.VMEM((1, D, ff), BF16),
            pltpu.VMEM((1, D, ff), BF16),
            pltpu.VMEM((1, ff, D), BF16),
            pltpu.VMEM((HALO + 16, width), BF16),
            pltpu.VMEM((HALO + 16, width), BF16),
            pltpu.VMEM((tokens + HALO, width), F32),
            pltpu.VMEM((32, width), F32),
            pltpu.VMEM((T, rows, width), BF16),
            pltpu.VMEM((T, rows, width), BF16),
            pltpu.VMEM((T, rows, width), BF16),
            pltpu.VMEM((rows, D), BF16),
            pltpu.VMEM((rows, D), BF16),
            pltpu.VMEM((E, cap, D), BF16),
            pltpu.VMEM((E, cap, D), BF16),
            pltpu.VMEM((cap, ff), BF16),
            pltpu.VMEM((E, cap, D), BF16),
            pltpu.VMEM((E, cap, D), BF16),
            dma((6,)),
            dma((S,)),
            dma((2,)),
            dma((Z,)),
            dma((Z,)),
            dma((S, Z)),
            dma((S, Z)),
            dma((Z,)),
            dma((Z,)),
            dma((T,)),
            dma((T,)),
            dma((S,)),
            dma((S,)),
            dma((S,)),
            dma((S,)),
        ],
        compiler_params=pltpu.CompilerParams(
            collective_id=0, has_side_effects=True, vmem_limit_bytes=60 * 1024 * 1024
        ),
    )(
        conv_value,
        conv_gate,
        least_tap,
        doc_ids,
        conv_kernel,
        norm_gain_conv[None, :],
        norm_bias_conv[None, :],
        proj_weight,
        residual,
        norm_gain_moe[None, :],
        group_router.T,
        expert_router.T,
        routing.T,
        expert_gate_w,
        expert_up_w,
        expert_down_w,
    )


def solution(mesh):
    placed = (
        P("sp", "tp"),
        P("sp", "tp"),
        P("sp"),
        P(None, "tp"),
        P(),
        P(),
        P("tp", None),
        P(("sp", "tp"), None),
        P(),
        P(),
        P(),
        P(("sp", "tp"), None),
        P("sp", None, None),
        P("sp", None, None),
        P("sp", None, None),
    )
    return jax.shard_map(
        functools.partial(body, mesh.shape["sp"], mesh.shape["tp"]),
        mesh=mesh,
        in_specs=placed,
        out_specs=P(("sp", "tp"), None),
        check_vma=False,
    )
```

profile of v0, /device:TPU:8, one launch (start us, length us, event | category | flops | bytes accessed | tf_op | source)
XLA Modules:
  0.0 108.6 jit_solution(16491196680561118078)
XLA Ops:
  0.0 1.8 %convert_reduce_fusion = s32[1536]{0:T(1024)S(1)} fusion(s32[1536]{0:T(1024)} %ids_ref.1), kind=kLoop, calls=%fused_computation | loop fusion | flops 7076352 | bytes 12288 | tf_op jit(solution)/shard_map/reduce_sum | solution.py:472
  1.9 1.1 %broadcast_in_dim.10.least_tap_ref = s32[1536,128]{1,0:T(8,128)} broadcast(s32[1536]{0:T(1024)S(1)} %subtract_select_fusion), dimensions={0} | broadcast | bytes 792576 | tf_op jit(solution)/shard_map/broadcast_in_dim | solution.py:475
  3.0 103.5 %shard_map.145 = bf16[192,2048]{1,0:T(8,128)(2,1)} custom-call(bf16[1536,256]{1,0:T(8,128)(2,1)} %value_hbm.1, bf16[1536,256]{1,0:T(8,128)(2,1)} %gate_hbm.1, s32[1536,128]{1,0:T(8,128)} %broadcast_in_dim.10.least_tap_ref, s32[1536]{0:T(1024)} %ids_ref.1, bf16[31,256]{1,0:T(8,128)(2,1)} %kernel_ref.1, f32[1,2048]{1,0:T(1,128)} %bitcast.7, ...), custom_call_target="tpu_custom_call" | custom-call | tf_op jit(solution)/shard_map/pallas_call | solution.py:482
  106.6 2.1 %copy.17 = bf16[192,2048]{1,0:T(8,128)(2,1)} copy(bf16[192,2048]{1,0:T(8,128)(2,1)} %shard_map.145) | data formatting | bytes 1572864
  (1 shorter events, 0.0 us)
where the time goes:
time: 109 us
  Pallas kernels  104 us (95%)
  local copies, waits for them, and re-layouts  3.24 us (3%)
  other arithmetic  1.85 us (2%)
    pallas_call x1, Pallas kernels, body(): pl.pallas_call(functools.partial(kernel, S, T, G), out_shape=jax.ShapeDty...  104 us

commit v1 on v0

--- a/solution.py
+++ b/solution.py
@@ -24,7 +24,7 @@
     G,
     value_hbm,
     gate_hbm,
-    least_tap_ref,
+    ids_row_ref,
     ids_ref,
     kernel_ref,
     gain_conv_ref,
@@ -50,11 +50,13 @@
     rim_in,
     padded,
     taps,
+    least_tap,
     conv_out,
     conv_in,
     act,
     hidden,
     normed,
+    picks,
     outgoing,
     arrived,
     ffn_hidden,
@@ -85,8 +87,12 @@
     tokens, width = value.shape
     block = tokens // T
     n_taps = kernel_ref.shape[0]
-    piece = wfull.shape[3]
+    piece = wfull.shape[2]
+    wrows = wfull.shape[1] // T
     D = S * piece
+    square = S == 4
+    H = 2
+    part_rows = wrows // H
 
     def remote(src, dst, send, recv, sp_to, tp_to):
         return pltpu.make_async_remote_copy(
@@ -111,9 +117,10 @@
             ]
         )
     ]
+    own_rows = pl.ds(pl.multiple_of(t * wrows, wrows), wrows)
     own_w = [
         pltpu.make_async_copy(
-            weight_hbm.at[:, pl.ds(j * piece, piece)], wfull.at[t, j], wl_sem.at[j]
+            weight_hbm.at[:, pl.ds(j * piece, piece)], wfull.at[j, own_rows, :], wl_sem.at[j]
         )
         for j in range(S)
     ]
@@ -124,34 +131,148 @@
     for c in loads[2:]:
         c.start()
 
-    barrier = pltpu.get_barrier_semaphore()
-    for k in range(1, T):
-        pl.semaphore_signal(
-            barrier, inc=1, device_id=(s, lax.rem(t + k, T)), device_id_type=MESH
-        )
-    for k in range(1, S):
-        pl.semaphore_signal(
-            barrier, inc=1, device_id=(lax.rem(s + k, S), t), device_id_type=MESH
-        )
-    pl.semaphore_wait(barrier, T + S - 2)
-
-    for c in own_w:
-        c.wait()
-    waits = []
-    for k in range(1, Z):
-        to = 2 * lax.rem(z + k, Z) + core
-        c = remote(wfull.at[t, s], wfull.at[t, s], wz_send.at[k], wz_recv.at[z], s, to)
-        c.start()
-        waits.append(c)
-    c = remote(wfull.at[t], wfull.at[t], wp_send.at[z], wp_recv.at[z], s, partner)
-    c.start()
-    waits.append(c)
+    ids_row = jnp.broadcast_to(ids_row_ref[...], (8, tokens))
+    position = lax.broadcasted_iota(jnp.int32, (8, tokens), 1)
+    low = jnp.int32(-n_taps)
+    fresh = (ids_row != pltpu.roll(ids_row, 1, 1)) & (position > 0)
+    begin = jnp.where(fresh, position, low)
+    shift = 1
+    while shift < n_taps:
+        moved = jnp.where(position >= shift, pltpu.roll(begin, shift, 1), low)
+        begin = jnp.maximum(begin, moved)
+        shift *= 2
+    least_row = (n_taps - 1 - position + begin).astype(F32)
+    lanes = least_tap.shape[1]
+    for c in range(tokens // lanes):
+        across = jnp.broadcast_to(least_row[0:1, c * lanes : (c + 1) * lanes], (lanes, lanes))
+        least_tap[c * lanes : (c + 1) * lanes, :] = across.T
+
+    with jax.named_scope("barrier"):
+        barrier = pltpu.get_barrier_semaphore()
+        for k in range(1, T):
+            pl.semaphore_signal(
+                barrier, inc=1, device_id=(s, lax.rem(t + k, T)), device_id_type=MESH
+            )
+        for k in range(1, S):
+            pl.semaphore_signal(
+                barrier, inc=1, device_id=(lax.rem(s + k, S), t), device_id_type=MESH
+            )
+        pl.semaphore_wait(barrier, T + S - 2)
+
+    def w_ref(o, p, h):
+        base = pl.multiple_of((2 * o + core) * wrows + h * part_rows, part_rows)
+        return wfull.at[p, pl.ds(base, part_rows), :]
+
+    def z_copy(o, h, up, to):
+        ref = w_ref(o, s, h)
+        return remote(ref, ref, wz_send.at[up, o, h], wz_recv.at[o, h], s, 2 * to + core)
+
+    def x_copy(o, p, h, lane_at, to):
+        ref = w_ref(o, p, h)
+        return remote(ref, ref, wx_send.at[lane_at, o, h], wx_recv.at[p, o, h], to, t)
+
+    def p_copy(o, p):
+        rows_at = pl.ds(pl.multiple_of((2 * o + core) * wrows, wrows), wrows)
+        ref = wfull.at[p, rows_at, :]
+        return remote(ref, ref, wp_send.at[o, p], wp_recv.at[o, p], s, partner)
+
+    def p_wait(o, p):
+        rows_at = pl.ds(pl.multiple_of((2 * o + 1 - core) * wrows, wrows), wrows)
+        ref = wfull.at[p, rows_at, :]
+        remote(ref, ref, wp_send.at[o, p], wp_recv.at[o, p], s, partner).wait_recv()
+
+    has_up = z + 1 < Z
+    has_down = z > 0
+    for j in range(S):
+        own_w[j].wait()
+    for h in range(H):
+
+        @pl.when(has_up)
+        def _():
+            z_copy(z, h, 0, z + 1).start()
+
+        @pl.when(has_down)
+        def _():
+            z_copy(z, h, 1, z - 1).start()
+
+    for j in range(S):
+        p_copy(z, j).start()
+
+    def sides(k):
+        return ((z - k, z - k >= 0, 0), (z + k, z + k < Z, 1))
+
+    def each_slice(k, act_on):
+        for o, there, side in sides(k):
+            pl.when(there)(functools.partial(act_on, o, side))
+
+    nbr_x = s + 1 - 2 * (s % 2)
+    nbr_y = s + 2 - 4 * (s // 2)
+    diag = 3 - s
+
+    def z_step(k, h):
+        def one(o, side):
+            z_copy(o, h, side, z).wait_recv()
+            beyond = has_down if side else has_up
+
+            @pl.when(beyond)
+            def _():
+                z_copy(o, h, side, z - 1 if side else z + 1).start()
+
+            if square:
+                x_copy(o, s, h, 0, nbr_x).start()
+                x_copy(o, s, h, 1, nbr_y).start()
+            else:
+                for j in range(1, S):
+                    x_copy(o, s, h, j - 1, lax.rem(s + j, S)).start()
+
+        with jax.named_scope(f"z{k}{h}"):
+            each_slice(k, one)
+
+    def x_step(k):
+        def one(o, side):
+            x_copy(o, nbr_x, 0, 2, nbr_y).wait_recv()
+            x_copy(o, nbr_x, 0, 2, nbr_y).start()
+
+        if square:
+            with jax.named_scope(f"x{k}"):
+                each_slice(k, one)
+
+    def y_step(k):
+        def one(o, side):
+            x_copy(o, nbr_y, 1, 2, nbr_x).wait_recv()
+            x_copy(o, nbr_y, 1, 2, nbr_x).start()
+
+        if square:
+            with jax.named_scope(f"y{k}"):
+                each_slice(k, one)
+
+    def finish_row(k):
+        def one(o, side):
+            p_copy(o, s).start()
+            if square:
+                x_copy(o, nbr_x, 1, 0, nbr_x).wait_recv()
+                p_copy(o, nbr_x).start()
+                x_copy(o, nbr_y, 0, 0, nbr_y).wait_recv()
+                p_copy(o, nbr_y).start()
+                x_copy(o, diag, 0, 0, diag).wait_recv()
+                x_copy(o, diag, 1, 0, diag).wait_recv()
+                p_copy(o, diag).start()
+            else:
+                for j in range(1, S):
+                    p = lax.rem(s + S - j, S)
+                    for h in range(H):
+                        x_copy(o, p, h, j - 1, p).wait_recv()
+                    p_copy(o, p).start()
+
+        with jax.named_scope(f"fin{k}"):
+            each_slice(k, one)
 
     loads[0].wait()
     loads[1].wait()
     tail = pl.ds(tokens - HALO, HALO)
-    last_reach = jnp.max(least_tap_ref[tokens - 1 : tokens, :], axis=1, keepdims=True)
-    newer = lax.broadcasted_iota(jnp.int32, (HALO, width), 0) >= last_reach + HALO - n_taps
+    last_reach = jnp.max(least_tap[tokens - 1 : tokens, :], axis=1, keepdims=True)
+    row_at = lax.broadcasted_iota(jnp.int32, (HALO, width), 0).astype(F32)
+    newer = row_at >= last_reach + (HALO - n_taps)
     rim = jnp.where(newer, gate(value[tail, :], gates[tail, :]).astype(F32), jnp.float32(0.0))
     rim_out[0:HALO, :] = rim.astype(BF16)
     rim_out[HALO : HALO + 16, :] = jnp.full(
@@ -168,11 +289,9 @@
         padded[to_rows, :] = gate(value[rows, :], gates[rows, :]).astype(F32)
         return 0
 
-    lax.fori_loop(0, tokens // 64, gate_rows, 0)
+    with jax.named_scope("gate"):
+        lax.fori_loop(0, tokens // 64, gate_rows, 0)
     taps[0:n_taps, :] = kernel_ref[...].astype(F32)
-    rim_copy.wait()
-    same = (rim_in[HALO : HALO + 1, :].astype(F32) == ids_ref[0].astype(F32)) & (s > 0)
-    padded[0:HALO, :] = jnp.where(same, rim_in[0:HALO, :].astype(F32), jnp.float32(0.0))
 
     step_rows = 32 if block % 32 == 0 else 8
     lanes = min(width, 128)
@@ -180,7 +299,7 @@
     def conv_block(owner):
         def conv_rows(i, _):
             base = pl.multiple_of(owner * block + i * step_rows, 8)
-            least = least_tap_ref[pl.ds(base, step_rows), :]
+            least = least_tap[pl.ds(base, step_rows), :]
             window = padded[pl.ds(base, step_rows + HALO), :]
             total = jnp.zeros((step_rows, width), F32)
             for tap in range(n_taps):
@@ -199,41 +318,48 @@
 
         lax.fori_loop(0, block // step_rows, conv_rows, 0)
 
-    def conv_send(k, _):
-        owner = lax.rem(t + k, T)
-        conv_block(owner)
-        remote(
-            conv_out.at[owner],
-            conv_in.at[t],
-            a2a_send.at[owner],
-            a2a_recv.at[t],
-            s,
-            owner,
-        ).start()
-        return 0
-
-    done = 1
-    for k in range(1, Z):
-        upto = T - 2 * (Z - 1 - k)
-        lax.fori_loop(done, upto, conv_send, 0)
-        done = upto
-        from_z = lax.rem(z - k + Z, Z)
-        row = 2 * from_z + core
-        remote(
-            wfull.at[row, s], wfull.at[row, s], wz_send.at[k], wz_recv.at[from_z], s, t
-        ).wait_recv()
-        for j in range(1, S):
-            c = remote(
-                wfull.at[row, s],
-                wfull.at[row, s],
-                wx_send.at[j, from_z],
-                wx_recv.at[s, from_z],
-                lax.rem(s + j, S),
-                t,
-            )
-            c.start()
-            waits.append(c)
-    conv_block(t)
+    def conv_some(first, last):
+        with jax.named_scope("conv"):
+
+            def one(owner, _):
+                conv_block(owner)
+                return 0
+
+            lax.fori_loop(first, last, one, 0)
+
+    def conv_copy(to):
+        return remote(
+            conv_out.at[to], conv_in.at[t], a2a_send.at[to], a2a_recv.at[t], s, to
+        )
+
+    def conv_flush(first, last):
+        def one(k, _):
+            owner = lax.rem(t + k, T)
+
+            @pl.when((owner >= first) & (owner < last))
+            def _():
+                conv_copy(owner).start()
+
+            return 0
+
+        lax.fori_loop(1, T, one, 0)
+
+    marks = [1 + (T - 1) * i // 7 for i in (3, 5, 7)]
+    conv_some(1, marks[0])
+    z_step(1, 0)
+    conv_some(marks[0], marks[1])
+    z_step(1, 1)
+    conv_some(marks[1], marks[2])
+    z_step(2, 0)
+    x_step(1)
+    with jax.named_scope("rimwait"):
+        rim_copy.wait()
+    same = (rim_in[HALO : HALO + 1, :].astype(F32) == ids_ref[0].astype(F32)) & (s > 0)
+    padded[0:HALO, :] = jnp.where(same, rim_in[0:HALO, :].astype(F32), jnp.float32(0.0))
+    conv_some(0, 1)
+    z_step(2, 1)
+    conv_flush(0, T)
+    y_step(1)
     conv_in[t, :, :] = conv_out[t, :, :]
 
     rows = block
@@ -256,72 +382,83 @@
     per_group = E // G
     group_low = lane_f * per_group
     in_group = (first >= group_low) & (first < group_low + per_group)
-    tri = lax.broadcasted_iota(jnp.int32, (rows, rows), 0) > lax.broadcasted_iota(
-        jnp.int32, (rows, rows), 1
-    )
+    row_i = lax.broadcasted_iota(jnp.int32, (rows, rows), 0)
+    col_i = lax.broadcasted_iota(jnp.int32, (rows, rows), 1)
     before = jnp.dot(
-        tri.astype(F32).astype(BF16),
+        (row_i > col_i).astype(F32).astype(BF16),
         chosen.astype(F32).astype(BF16),
         preferred_element_type=F32,
     )
     slot = jnp.where(chosen, before, jnp.float32(-1.0))
-
-    for k in range(1, T):
-        source = lax.rem(t + k, T)
-        remote(
-            conv_out.at[source], conv_in.at[source], a2a_send.at[source], a2a_recv.at[source], s, source
-        ).wait_recv()
+    width_e = max(E, 8)
+    expert_i = lax.broadcasted_iota(jnp.int32, (width_e, rows), 0)
+    chosen_r = (routing_ref[0:1, :] == expert_i) | (routing_ref[1:2, :] == expert_i)
+    before_r = jnp.dot(
+        chosen_r.astype(F32).astype(BF16),
+        (row_i < col_i).astype(F32).astype(BF16),
+        preferred_element_type=F32,
+    )
+    slot_r = jnp.where(chosen_r, before_r, jnp.float32(-1.0))
+    cap_i = lax.broadcasted_iota(jnp.int32, (cap, rows), 0).astype(F32)
+    for e in range(E):
+        picks[e, :, :] = (slot_r[e : e + 1, :] == cap_i).astype(F32).astype(BF16)
+
+    for k in range(3, Z):
+        z_step(k, 0)
+        x_step(k - 1)
+        z_step(k, 1)
+        finish_row(k - 2)
+        y_step(k - 1)
+    finish_row(Z - 2)
+    x_step(Z - 1)
+    y_step(Z - 1)
+
     total = jnp.zeros((rows, 1), F32)
-    for j in range(T):
-        total = total + jnp.sum(conv_in[j].astype(F32), axis=1, keepdims=True)
-    average = total / (T * width)
-    total = jnp.zeros((rows, 1), F32)
-    for j in range(T):
-        centered = conv_in[j].astype(F32) - average
-        total = total + jnp.sum(centered * centered, axis=1, keepdims=True)
-    scale = lax.rsqrt(total / (T * width) + epsilon)
-    for j in range(T):
-        cols = slice(j * width, (j + 1) * width)
-        v = (conv_in[j].astype(F32) - average) * scale * gain_conv_ref[:, cols] + bias_conv_ref[
-            :, cols
-        ]
-        act[j, :, :] = (v / (1.0 + jnp.exp(-v))).astype(BF16)
-
-    for k in range(1, Z):
-        from_z = lax.rem(z - k + Z, Z)
-        row = 2 * from_z + core
-        for j in range(1, S):
-            source = lax.rem(s - j + S, S)
+    with jax.named_scope("a2await"):
+        for k in range(1, T):
+            source = lax.rem(t + k, T)
             remote(
-                wfull.at[row, source],
-                wfull.at[row, source],
-                wx_send.at[j, from_z],
-                wx_recv.at[source, from_z],
+                conv_out.at[source],
+                conv_in.at[source],
+                a2a_send.at[source],
+                a2a_recv.at[source],
+                s,
                 source,
-                t,
             ).wait_recv()
-        c = remote(
-            wfull.at[row], wfull.at[row], wp_send.at[from_z], wp_recv.at[from_z], s, partner
-        )
-        c.start()
-        waits.append(c)
+    with jax.named_scope("act"):
+        for j in range(T):
+            total = total + jnp.sum(conv_in[j].astype(F32), axis=1, keepdims=True)
+        average = total / (T * width)
+        total = jnp.zeros((rows, 1), F32)
+        for j in range(T):
+            centered = conv_in[j].astype(F32) - average
+            total = total + jnp.sum(centered * centered, axis=1, keepdims=True)
+        scale = lax.rsqrt(total / (T * width) + epsilon)
+        for j in range(T):
+            cols = slice(j * width, (j + 1) * width)
+            v = (conv_in[j].astype(F32) - average) * scale * gain_conv_ref[
+                :, cols
+            ] + bias_conv_ref[:, cols]
+            act[:, cols] = (v / (1.0 + jnp.exp(-v))).astype(BF16)
+
+    finish_row(Z - 1)
     loads[2].wait()
-    for j in range(Z):
-        row = 2 * j + 1 - core
-        remote(wfull.at[row], wfull.at[row], wp_send.at[j], wp_recv.at[j], s, partner).wait_recv()
+    with jax.named_scope("wpwait"):
+        for o in range(Z):
+            for j in range(S):
+                p_wait(o, j)
 
     def project(j, squares):
         cols = pl.ds(pl.multiple_of(j * piece, piece), piece)
         acc = residual[:, cols].astype(F32)
-        part = jnp.zeros_like(acc)
-        for i in range(T):
-            part = part + jnp.dot(act[i], wfull[i, j], preferred_element_type=F32)
+        part = jnp.dot(act[...], wfull[j], preferred_element_type=F32)
         state = (acc + part).astype(BF16)
         hidden[:, cols] = state
         state = state.astype(F32)
         return squares + jnp.sum(state * state, axis=1, keepdims=True)
 
-    squares = lax.fori_loop(0, S, project, jnp.zeros((rows, 1), F32))
+    with jax.named_scope("project"):
+        squares = lax.fori_loop(0, S, project, jnp.zeros((rows, 1), F32))
     scale = lax.rsqrt(squares / D + epsilon)
 
     def norm_cols(j, _):
@@ -329,7 +466,8 @@
         normed[:, cols] = (hidden[:, cols].astype(F32) * scale * gain_moe_ref[:, cols]).astype(BF16)
         return 0
 
-    lax.fori_loop(0, S, norm_cols, 0)
+    with jax.named_scope("norm"):
+        lax.fori_loop(0, S, norm_cols, 0)
 
     slot_iota = lax.broadcasted_iota(jnp.int32, (rows, cap), 1).astype(F32)
 
@@ -338,27 +476,23 @@
         return jnp.sum(jnp.where(mine, array, jnp.float32(0.0)), axis=1, keepdims=True)
 
     def gather_rows(expert, target):
-        picks = (column(slot, expert) == slot_iota).astype(F32).astype(BF16)
-
         def cols_step(j, _):
             cols = pl.ds(pl.multiple_of(j * piece, piece), piece)
-            target[:, cols] = lax.dot_general(
-                picks,
-                normed[:, cols],
-                (((0,), (0,)), ((), ())),
-                preferred_element_type=F32,
+            target[:, cols] = jnp.dot(
+                picks[expert], normed[:, cols], preferred_element_type=F32
             ).astype(BF16)
             return 0
 
         lax.fori_loop(0, S, cols_step, 0)
 
-    for k in range(1, S):
-        expert = lax.rem(s + k, S)
-        gather_rows(expert, outgoing.at[expert])
-        remote(
-            outgoing.at[expert], arrived.at[s], disp_send.at[expert], disp_recv.at[s], expert, t
-        ).start()
-    gather_rows(s, arrived.at[s])
+    with jax.named_scope("dispatch"):
+        for k in range(1, S):
+            expert = lax.rem(s + k, S)
+            gather_rows(expert, outgoing.at[expert])
+            remote(
+                outgoing.at[expert], arrived.at[s], disp_send.at[expert], disp_recv.at[s], expert, t
+            ).start()
+        gather_rows(s, arrived.at[s])
 
     def logits(router):
         return lax.dot_general(
@@ -399,7 +533,8 @@
 
         lax.fori_loop(0, S, down_step, 0)
 
-    expert_block(s, returned.at[s])
+    with jax.named_scope("ffnown"):
+        expert_block(s, returned.at[s])
     for k in range(1, S):
         sender = lax.rem(s - k + S, S)
         remote(
@@ -428,17 +563,47 @@
         out_ref[:, cols] = (hidden[:, cols].astype(F32) + acc).astype(BF16)
         return 0
 
-    lax.fori_loop(0, S, combine, 0)
-
-    for c in waits:
-        c.wait_send()
-    for k in range(1, T):
-        to = lax.rem(t + k, T)
-        remote(conv_out.at[to], conv_in.at[t], a2a_send.at[to], a2a_recv.at[t], s, to).wait_send()
-    for k in range(1, S):
-        to = lax.rem(s + k, S)
-        remote(outgoing.at[to], arrived.at[s], disp_send.at[to], disp_recv.at[s], to, t).wait_send()
-        remote(results.at[to], returned.at[s], ret_send.at[to], ret_recv.at[s], to, t).wait_send()
+    with jax.named_scope("combine"):
+        lax.fori_loop(0, S, combine, 0)
+
+    with jax.named_scope("sendwait"):
+        for h in range(H):
+
+            @pl.when(has_up)
+            def _():
+                z_copy(z, h, 0, z + 1).wait_send()
+
+            @pl.when(has_down)
+            def _():
+                z_copy(z, h, 1, z - 1).wait_send()
+
+        for j in range(S):
+            p_copy(z, j).wait_send()
+        def sent(o, side):
+            beyond = has_down if side else has_up
+            for h in range(H):
+
+                @pl.when(beyond)
+                def _():
+                    z_copy(o, h, side, z - 1 if side else z + 1).wait_send()
+
+                for j in range(3 if square else S - 1):
+                    x_copy(o, s, h, j, lax.rem(s + 1, S)).wait_send()
+            for j in range(S):
+                p_copy(o, j).wait_send()
+
+        for k in range(1, Z):
+            each_slice(k, sent)
+        for k in range(1, T):
+            conv_copy(lax.rem(t + k, T)).wait_send()
+        for k in range(1, S):
+            to = lax.rem(s + k, S)
+            remote(
+                outgoing.at[to], arrived.at[s], disp_send.at[to], disp_recv.at[s], to, t
+            ).wait_send()
+            remote(
+                results.at[to], returned.at[s], ret_send.at[to], ret_recv.at[s], to, t
+            ).wait_send()
 
 
 def body(
@@ -461,18 +626,12 @@
     expert_down_w,
 ):
     tokens, width = conv_value.shape
-    n_taps = conv_kernel.shape[0]
     rows, D = residual.shape
     wrows = proj_weight.shape[0]
     ff = expert_gate_w.shape[2]
     G = group_router.shape[1]
     E = expert_router.shape[1]
     cap = 2 * rows // E
-    lanes = min(width, 128)
-    start = jnp.sum((doc_ids[None, :] < doc_ids[:, None]).astype(jnp.int32), axis=1)
-    position = jnp.arange(tokens, dtype=jnp.int32)
-    least = jnp.where(start == 0, 0, n_taps - 1 - (position - start))
-    least_tap = jnp.broadcast_to(least[:, None], (tokens, lanes))
     vmem = pl.BlockSpec(memory_space=pltpu.VMEM)
     hbm = pl.BlockSpec(memory_space=pl.ANY)
     smem = pl.BlockSpec(memory_space=pltpu.SMEM)
@@ -490,7 +649,7 @@
         scratch_shapes=[
             pltpu.VMEM((tokens, width), BF16),
             pltpu.VMEM((tokens, width), BF16),
-            pltpu.VMEM((T, S, wrows, piece), BF16),
+            pltpu.VMEM((S, T * wrows, piece), BF16),
             pltpu.VMEM((rows, D), BF16),
             pltpu.VMEM((1, D, ff), BF16),
             pltpu.VMEM((1, D, ff), BF16),
@@ -499,11 +658,13 @@
             pltpu.VMEM((HALO + 16, width), BF16),
             pltpu.VMEM((tokens + HALO, width), F32),
             pltpu.VMEM((32, width), F32),
+            pltpu.VMEM((tokens, 128), F32),
             pltpu.VMEM((T, rows, width), BF16),
             pltpu.VMEM((T, rows, width), BF16),
-            pltpu.VMEM((T, rows, width), BF16),
+            pltpu.VMEM((rows, T * width), BF16),
             pltpu.VMEM((rows, D), BF16),
             pltpu.VMEM((rows, D), BF16),
+            pltpu.VMEM((E, cap, rows), BF16),
             pltpu.VMEM((E, cap, D), BF16),
             pltpu.VMEM((E, cap, D), BF16),
             pltpu.VMEM((cap, ff), BF16),
@@ -512,12 +673,12 @@
             dma((6,)),
             dma((S,)),
             dma((2,)),
-            dma((Z,)),
-            dma((Z,)),
-            dma((S, Z)),
-            dma((S, Z)),
-            dma((Z,)),
-            dma((Z,)),
+            dma((2, Z, 2)),
+            dma((Z, 2)),
+            dma((max(S - 1, 3), Z, 2)),
+            dma((S, Z, 2)),
+            dma((Z, S)),
+            dma((Z, S)),
             dma((T,)),
             dma((T,)),
             dma((S,)),
@@ -531,7 +692,7 @@
     )(
         conv_value,
         conv_gate,
-        least_tap,
+        doc_ids[None, :],
         doc_ids,
         conv_kernel,
         norm_gain_conv[None, :],

time: 109 us -> 97.8 us (0.90)
  the two profiles are of different devices: /device:TPU:8 before, /device:TPU:0 now
where the time goes in v1:
time: 97.8 us; the launch traced here: 97.5 us
  Pallas kernels  94.1 us (96%)
  local copies, waits for them, and re-layouts  3.38 us (3%)
    pallas_call x1, Pallas kernels, body(): pl.pallas_call(functools.partial(kernel, S, T, G), out_shape=jax.ShapeDty...  94.1 us
    unnamed x1, local copies, waits for them, and re-layouts  2.09 us

profile of v1, /device:TPU:0, one launch (start us, length us, event | category | flops | bytes accessed | tf_op | source)
XLA Modules:
  0.0 97.5 jit_solution(14619121141325267169)
XLA Ops:
  0.0 1.3 %broadcast_in_dim.12.ids_row_ref = s32[1,1536]{1,0:T(1,128)} reshape(s32[1536]{0:T(1024)} %ids_ref.1) | data formatting | bytes 12288 | tf_op jit(solution)/shard_map/broadcast_in_dim | solution.py:695
  1.3 94.1 %shard_map.145 = bf16[192,2048]{1,0:T(8,128)(2,1)} custom-call(bf16[1536,256]{1,0:T(8,128)(2,1)} %value_hbm.1, bf16[1536,256]{1,0:T(8,128)(2,1)} %gate_hbm.1, s32[1,1536]{1,0:T(1,128)} %broadcast_in_dim.12.ids_row_ref, s32[1536]{0:T(1024)} %ids_ref.1, bf16[31,256]{1,0:T(8,128)(2,1)} %kernel_ref.1, f32[1,2048]{1,0:T(1,128)} %bitcast.7, f32[1,2048]{1,0:T(1,128)} %bitcast.8, ...), custom_call_target="tpu_custom_call" | custom-call | tf_op jit(solution)/shard_map/pallas_call | solution.py:641
  95.4 2.1 %copy.17 = bf16[192,2048]{1,0:T(8,128)(2,1)} copy(bf16[192,2048]{1,0:T(8,128)(2,1)} %shard_map.145) | data formatting | bytes 1572864

commit v2 on v1

--- a/solution.py
+++ b/solution.py
@@ -56,7 +56,9 @@
     act,
     hidden,
     normed,
+    normed_in,
     picks,
+    spreads,
     outgoing,
     arrived,
     ffn_hidden,
@@ -77,6 +79,7 @@
     disp_recv,
     ret_send,
     ret_recv,
+    out_sem,
 ):
     s = lax.axis_index("sp")
     t = lax.axis_index("tp")
@@ -332,17 +335,15 @@
             conv_out.at[to], conv_in.at[t], a2a_send.at[to], a2a_recv.at[t], s, to
         )
 
-    def conv_flush(first, last):
-        def one(k, _):
-            owner = lax.rem(t + k, T)
-
-            @pl.when((owner >= first) & (owner < last))
-            def _():
-                conv_copy(owner).start()
-
-            return 0
-
-        lax.fori_loop(1, T, one, 0)
+    def conv_flush():
+        conv_copy(partner).start()
+        for far in range(1, Z):
+            for to, there, _ in sides(far):
+
+                @pl.when(there)
+                def _():
+                    for c in range(2):
+                        conv_copy(2 * to + c).start()
 
     marks = [1 + (T - 1) * i // 7 for i in (3, 5, 7)]
     conv_some(1, marks[0])
@@ -358,7 +359,7 @@
     padded[0:HALO, :] = jnp.where(same, rim_in[0:HALO, :].astype(F32), jnp.float32(0.0))
     conv_some(0, 1)
     z_step(2, 1)
-    conv_flush(0, T)
+    conv_flush()
     y_step(1)
     conv_in[t, :, :] = conv_out[t, :, :]
 
@@ -448,119 +449,167 @@
             for j in range(S):
                 p_wait(o, j)
 
+    others = [nbr_x, nbr_y, diag] if square else [lax.rem(s + S - k, S) for k in range(1, S)]
+    prompt = others[:2] if square else others
+    late = others[2:] if square else []
+
+    def disp_copy(expert, j):
+        return remote(
+            outgoing.at[expert, j],
+            arrived.at[s, j],
+            disp_send.at[expert, j],
+            disp_recv.at[s, j],
+            expert,
+            t,
+        )
+
+    def disp_wait(sender, j):
+        remote(
+            outgoing.at[sender, j],
+            arrived.at[sender, j],
+            disp_send.at[sender, j],
+            disp_recv.at[sender, j],
+            sender,
+            t,
+        ).wait_recv()
+
+    def ret_copy(sender, j):
+        return remote(
+            results.at[sender, j],
+            returned.at[s, j],
+            ret_send.at[sender, j],
+            ret_recv.at[s, j],
+            sender,
+            t,
+        )
+
+    def ret_wait(expert, j):
+        remote(
+            results.at[expert, j],
+            returned.at[expert, j],
+            ret_send.at[expert, j],
+            ret_recv.at[expert, j],
+            expert,
+            t,
+        ).wait_recv()
+
+    def piece_cols(j):
+        return pl.ds(pl.multiple_of(j * piece, piece), piece)
+
     def project(j, squares):
-        cols = pl.ds(pl.multiple_of(j * piece, piece), piece)
+        cols = piece_cols(j)
         acc = residual[:, cols].astype(F32)
         part = jnp.dot(act[...], wfull[j], preferred_element_type=F32)
         state = (acc + part).astype(BF16)
         hidden[:, cols] = state
+        for expert in others:
+            outgoing[expert, j, :, :] = jnp.dot(
+                picks[expert], state, preferred_element_type=F32
+            ).astype(BF16)
+        for expert in prompt:
+            disp_copy(expert, j).start()
+        arrived[s, j, :, :] = jnp.dot(picks[s], state, preferred_element_type=F32).astype(BF16)
         state = state.astype(F32)
         return squares + jnp.sum(state * state, axis=1, keepdims=True)
 
     with jax.named_scope("project"):
         squares = lax.fori_loop(0, S, project, jnp.zeros((rows, 1), F32))
+        for expert in late:
+            for j in range(S):
+                disp_copy(expert, j).start()
+
+    for c in loads[3:]:
+        c.wait()
+    ff = gate_w.shape[2]
+    ff_step = min(ff, 256)
+
+    def expert_block(sender, target, send):
+        def square_step(j, squares):
+            x = arrived[sender, j].astype(F32)
+            return squares + jnp.sum(x * x, axis=1, keepdims=True)
+
+        total = lax.fori_loop(0, S, square_step, jnp.zeros((cap, 1), F32))
+        row_scale = lax.rsqrt(total / D + epsilon)
+
+        def norm_step(j, _):
+            cols = piece_cols(j)
+            x = arrived[sender, j].astype(F32)
+            normed_in[:, cols] = (x * row_scale * gain_moe_ref[:, cols]).astype(BF16)
+            return 0
+
+        lax.fori_loop(0, S, norm_step, 0)
+
+        def up_step(j, _):
+            cols = pl.ds(pl.multiple_of(j * ff_step, ff_step), ff_step)
+            x = normed_in[...]
+            g = jnp.dot(x, gate_w[0, :, cols], preferred_element_type=F32)
+            u = jnp.dot(x, up_w[0, :, cols], preferred_element_type=F32)
+            ffn_hidden[:, cols] = (g / (1.0 + jnp.exp(-g)) * u).astype(BF16)
+            return 0
+
+        lax.fori_loop(0, ff // ff_step, up_step, 0)
+
+        def down_step(j, _):
+            target[j, :, :] = jnp.dot(
+                ffn_hidden[...], down_w[0, :, piece_cols(j)], preferred_element_type=F32
+            ).astype(BF16)
+            if send:
+                ret_copy(sender, j).start()
+            return 0
+
+        lax.fori_loop(0, S, down_step, 0)
+
+    with jax.named_scope("ffnown"):
+        expert_block(s, returned.at[s], False)
+
     scale = lax.rsqrt(squares / D + epsilon)
 
     def norm_cols(j, _):
-        cols = pl.ds(pl.multiple_of(j * piece, piece), piece)
+        cols = piece_cols(j)
         normed[:, cols] = (hidden[:, cols].astype(F32) * scale * gain_moe_ref[:, cols]).astype(BF16)
         return 0
-
-    with jax.named_scope("norm"):
-        lax.fori_loop(0, S, norm_cols, 0)
-
-    slot_iota = lax.broadcasted_iota(jnp.int32, (rows, cap), 1).astype(F32)
-
-    def column(array, expert):
-        mine = lane[:, : array.shape[1]] == expert
-        return jnp.sum(jnp.where(mine, array, jnp.float32(0.0)), axis=1, keepdims=True)
-
-    def gather_rows(expert, target):
-        def cols_step(j, _):
-            cols = pl.ds(pl.multiple_of(j * piece, piece), piece)
-            target[:, cols] = jnp.dot(
-                picks[expert], normed[:, cols], preferred_element_type=F32
-            ).astype(BF16)
-            return 0
-
-        lax.fori_loop(0, S, cols_step, 0)
-
-    with jax.named_scope("dispatch"):
-        for k in range(1, S):
-            expert = lax.rem(s + k, S)
-            gather_rows(expert, outgoing.at[expert])
-            remote(
-                outgoing.at[expert], arrived.at[s], disp_send.at[expert], disp_recv.at[s], expert, t
-            ).start()
-        gather_rows(s, arrived.at[s])
 
     def logits(router):
         return lax.dot_general(
             normed[...], router[...], (((1,), (1,)), ((), ())), preferred_element_type=F32
         )
 
-    group_exp = jnp.exp(logits(group_router_ref))
-    expert_exp = jnp.exp(logits(expert_router_ref))
+    def column(array, expert):
+        mine = lane[:, : array.shape[1]] == expert
+        return jnp.sum(jnp.where(mine, array, jnp.float32(0.0)), axis=1, keepdims=True)
+
     zero = jnp.float32(0.0)
-    group_prob = jnp.sum(
-        jnp.where(in_group[:, :G], group_exp, zero), axis=1, keepdims=True
-    ) / jnp.sum(group_exp, axis=1, keepdims=True)
-    chosen_exp = jnp.where(chosen[:, :E], expert_exp, zero)
-    mix = group_prob * chosen_exp / jnp.sum(chosen_exp, axis=1, keepdims=True)
-
-    for c in loads[3:]:
-        c.wait()
-    ff = gate_w.shape[2]
-    ff_step = min(ff, 256)
-
-    def expert_block(sender, target):
-        def up_step(j, _):
-            cols = pl.ds(pl.multiple_of(j * ff_step, ff_step), ff_step)
-            x = arrived[sender]
-            g = jnp.dot(x, gate_w[0, :, cols], preferred_element_type=F32)
-            u = jnp.dot(x, up_w[0, :, cols], preferred_element_type=F32)
-            ffn_hidden[:, cols] = (g / (1.0 + jnp.exp(-g)) * u).astype(BF16)
-            return 0
-
-        lax.fori_loop(0, ff // ff_step, up_step, 0)
-
-        def down_step(j, _):
-            cols = pl.ds(pl.multiple_of(j * piece, piece), piece)
-            target[:, cols] = jnp.dot(
-                ffn_hidden[...], down_w[0, :, cols], preferred_element_type=F32
+    with jax.named_scope("router"):
+        lax.fori_loop(0, S, norm_cols, 0)
+        group_exp = jnp.exp(logits(group_router_ref))
+        expert_exp = jnp.exp(logits(expert_router_ref))
+        group_prob = jnp.sum(
+            jnp.where(in_group[:, :G], group_exp, zero), axis=1, keepdims=True
+        ) / jnp.sum(group_exp, axis=1, keepdims=True)
+        chosen_exp = jnp.where(chosen[:, :E], expert_exp, zero)
+        mix = group_prob * chosen_exp / jnp.sum(chosen_exp, axis=1, keepdims=True)
+        slot_iota = lax.broadcasted_iota(jnp.int32, (rows, cap), 1).astype(F32)
+        for e in range(E):
+            spreads[e, :, :] = jnp.where(
+                column(slot, e) == slot_iota, column(mix, e), zero
             ).astype(BF16)
-            return 0
-
-        lax.fori_loop(0, S, down_step, 0)
-
-    with jax.named_scope("ffnown"):
-        expert_block(s, returned.at[s])
-    for k in range(1, S):
-        sender = lax.rem(s - k + S, S)
-        remote(
-            outgoing.at[sender], arrived.at[sender], disp_send.at[sender], disp_recv.at[sender], sender, t
-        ).wait_recv()
-        expert_block(sender, results.at[sender])
-        remote(
-            results.at[sender], returned.at[s], ret_send.at[sender], ret_recv.at[s], sender, t
-        ).start()
-
-    for k in range(1, S):
-        expert = lax.rem(s + k, S)
-        remote(
-            results.at[expert], returned.at[expert], ret_send.at[expert], ret_recv.at[expert], expert, t
-        ).wait_recv()
-    spreads = [
-        jnp.where(column(slot, e) == slot_iota, column(mix, e), zero).astype(BF16)
-        for e in range(E)
-    ]
+
+    for i, sender in enumerate(others):
+        with jax.named_scope(f"dispwait{i}"):
+            for j in range(S):
+                disp_wait(sender, j)
+        with jax.named_scope(f"ffn{i}"):
+            expert_block(sender, results.at[sender], True)
 
     def combine(j, _):
-        cols = pl.ds(pl.multiple_of(j * piece, piece), piece)
-        acc = jnp.zeros((rows, piece), F32)
+        cols = piece_cols(j)
+        for expert in others:
+            ret_wait(expert, j)
+        acc = hidden[:, cols].astype(F32)
         for e in range(E):
-            acc = acc + jnp.dot(spreads[e], returned[e, :, cols], preferred_element_type=F32)
-        out_ref[:, cols] = (hidden[:, cols].astype(F32) + acc).astype(BF16)
+            acc = acc + jnp.dot(spreads[e], returned[e, j], preferred_element_type=F32)
+        hidden[:, cols] = acc.astype(BF16)
+        pltpu.make_async_copy(hidden.at[:, cols], out_ref.at[:, cols], out_sem.at[j]).start()
         return 0
 
     with jax.named_scope("combine"):
@@ -596,14 +645,13 @@
             each_slice(k, sent)
         for k in range(1, T):
             conv_copy(lax.rem(t + k, T)).wait_send()
-        for k in range(1, S):
-            to = lax.rem(s + k, S)
-            remote(
-                outgoing.at[to], arrived.at[s], disp_send.at[to], disp_recv.at[s], to, t
-            ).wait_send()
-            remote(
-                results.at[to], returned.at[s], ret_send.at[to], ret_recv.at[s], to, t
-            ).wait_send()
+        for expert in others:
+            for j in range(S):
+                disp_copy(expert, j).wait_send()
+                ret_copy(expert, j).wait_send()
+        for j in range(S):
+            cols = piece_cols(j)
+            pltpu.make_async_copy(hidden.at[:, cols], out_ref.at[:, cols], out_sem.at[j]).wait()
 
 
 def body(
@@ -645,7 +693,7 @@
             hbm, hbm, vmem, smem, vmem, vmem, vmem, hbm, hbm, vmem, vmem, vmem, vmem,
             hbm, hbm, hbm,
         ],
-        out_specs=vmem,
+        out_specs=hbm,
         scratch_shapes=[
             pltpu.VMEM((tokens, width), BF16),
             pltpu.VMEM((tokens, width), BF16),
@@ -664,12 +712,14 @@
             pltpu.VMEM((rows, T * width), BF16),
             pltpu.VMEM((rows, D), BF16),
             pltpu.VMEM((rows, D), BF16),
+            pltpu.VMEM((cap, D), BF16),
             pltpu.VMEM((E, cap, rows), BF16),
-            pltpu.VMEM((E, cap, D), BF16),
-            pltpu.VMEM((E, cap, D), BF16),
+            pltpu.VMEM((E, rows, cap), BF16),
+            pltpu.VMEM((E, S, cap, piece), BF16),
+            pltpu.VMEM((E, S, cap, piece), BF16),
             pltpu.VMEM((cap, ff), BF16),
-            pltpu.VMEM((E, cap, D), BF16),
-            pltpu.VMEM((E, cap, D), BF16),
+            pltpu.VMEM((E, S, cap, piece), BF16),
+            pltpu.VMEM((E, S, cap, piece), BF16),
             dma((6,)),
             dma((S,)),
             dma((2,)),
@@ -681,9 +731,10 @@
             dma((Z, S)),
             dma((T,)),
             dma((T,)),
-            dma((S,)),
-            dma((S,)),
-            dma((S,)),
+            dma((S, S)),
+            dma((S, S)),
+            dma((S, S)),
+            dma((S, S)),
             dma((S,)),
         ],
         compiler_params=pltpu.CompilerParams(

time: 97.8 us -> 85.6 us (0.88)
  Pallas kernels: 94.1 us -> 82 us
    pallas_call x1, Pallas kernels: 94.1 us -> 82 us  [body(): pl.pallas_call(functools.partial(kernel, S, T, G), out_shape=jax.ShapeDty...]
where the time goes in v2:
time: 85.6 us; the launch traced here: 85.4 us
  Pallas kernels  82 us (96%)
  local copies, waits for them, and re-layouts  3.38 us (4%)
    pallas_call x1, Pallas kernels, body(): pl.pallas_call(functools.partial(kernel, S, T, G), out_shape=jax.ShapeDty...  82 us
    unnamed x1, local copies, waits for them, and re-layouts  2.09 us

profile of v2, /device:TPU:0, one launch (start us, length us, event | category | flops | bytes accessed | tf_op | source)
XLA Modules:
  0.0 85.4 jit_solution(2354878671424697459)
XLA Ops:
  0.0 1.3 %broadcast_in_dim.12.ids_row_ref = s32[1,1536]{1,0:T(1,128)} reshape(s32[1536]{0:T(1024)} %ids_ref.1) | data formatting | bytes 12288 | tf_op jit(solution)/shard_map/broadcast_in_dim | solution.py:746
  1.3 82.0 %shard_map.145 = bf16[192,2048]{1,0:T(8,128)(2,1)} custom-call(bf16[1536,256]{1,0:T(8,128)(2,1)} %value_hbm.1, bf16[1536,256]{1,0:T(8,128)(2,1)} %gate_hbm.1, s32[1,1536]{1,0:T(1,128)} %broadcast_in_dim.12.ids_row_ref, s32[1536]{0:T(1024)} %ids_ref.1, bf16[31,256]{1,0:T(8,128)(2,1)} %kernel_ref.1, f32[1,2048]{1,0:T(1,128)} %bitcast.7, f32[1,2048]{1,0:T(1,128)} %bitcast.8, ...), custom_call_target="tpu_custom_call" | custom-call | tf_op jit(solution)/shard_map/pallas_call | solution.py:689
  83.3 2.1 %copy.17 = bf16[192,2048]{1,0:T(8,128)(2,1)} copy(bf16[192,2048]{1,0:T(8,128)(2,1)} %shard_map.145) | data formatting | bytes 1572864

commit v3 on v2

--- a/solution.py
+++ b/solution.py
@@ -24,21 +24,28 @@
     G,
     value_hbm,
     gate_hbm,
+    ids_hbm,
+    kernel_hbm,
+    gain_conv_hbm,
+    bias_conv_hbm,
+    weight_hbm,
+    residual_hbm,
+    gain_moe_hbm,
+    group_router_hbm,
+    expert_router_hbm,
+    routing_hbm,
+    gate_w_hbm,
+    up_w_hbm,
+    down_w_hbm,
+    out_ref,
     ids_row_ref,
-    ids_ref,
     kernel_ref,
     gain_conv_ref,
     bias_conv_ref,
-    weight_hbm,
-    residual_hbm,
     gain_moe_ref,
     group_router_ref,
     expert_router_ref,
     routing_ref,
-    gate_w_hbm,
-    up_w_hbm,
-    down_w_hbm,
-    out_ref,
     value,
     gates,
     wfull,
@@ -79,7 +86,6 @@
     disp_recv,
     ret_send,
     ret_recv,
-    out_sem,
 ):
     s = lax.axis_index("sp")
     t = lax.axis_index("tp")
@@ -107,13 +113,31 @@
             device_id_type=MESH,
         )
 
+    barrier = pltpu.get_barrier_semaphore()
+    for k in range(1, T):
+        pl.semaphore_signal(
+            barrier, inc=1, device_id=(s, lax.rem(t + k, T)), device_id_type=MESH
+        )
+    for k in range(1, S):
+        pl.semaphore_signal(
+            barrier, inc=1, device_id=(lax.rem(s + k, S), t), device_id_type=MESH
+        )
+
     loads = [
         pltpu.make_async_copy(a, b, local_sem.at[i])
         for i, (a, b) in enumerate(
             [
+                (ids_hbm, ids_row_ref),
                 (value_hbm, value),
                 (gate_hbm, gates),
+                (kernel_hbm, kernel_ref),
+                (routing_hbm, routing_ref),
+                (gain_conv_hbm, gain_conv_ref),
+                (bias_conv_hbm, bias_conv_ref),
                 (residual_hbm, residual),
+                (gain_moe_hbm, gain_moe_ref),
+                (group_router_hbm, group_router_ref),
+                (expert_router_hbm, expert_router_ref),
                 (gate_w_hbm, gate_w),
                 (up_w_hbm, up_w),
                 (down_w_hbm, down_w),
@@ -128,12 +152,12 @@
         for j in range(S)
     ]
     loads[0].start()
-    loads[1].start()
     for c in own_w:
         c.start()
-    for c in loads[2:]:
+    for c in loads[1:]:
         c.start()
 
+    loads[0].wait()
     ids_row = jnp.broadcast_to(ids_row_ref[...], (8, tokens))
     position = lax.broadcasted_iota(jnp.int32, (8, tokens), 1)
     low = jnp.int32(-n_taps)
@@ -151,15 +175,6 @@
         least_tap[c * lanes : (c + 1) * lanes, :] = across.T
 
     with jax.named_scope("barrier"):
-        barrier = pltpu.get_barrier_semaphore()
-        for k in range(1, T):
-            pl.semaphore_signal(
-                barrier, inc=1, device_id=(s, lax.rem(t + k, T)), device_id_type=MESH
-            )
-        for k in range(1, S):
-            pl.semaphore_signal(
-                barrier, inc=1, device_id=(lax.rem(s + k, S), t), device_id_type=MESH
-            )
         pl.semaphore_wait(barrier, T + S - 2)
 
     def w_ref(o, p, h):
@@ -211,6 +226,7 @@
     nbr_x = s + 1 - 2 * (s % 2)
     nbr_y = s + 2 - 4 * (s // 2)
     diag = 3 - s
+    order = [s, nbr_x, nbr_y, diag] if square else [lax.rem(s + S - j, S) for j in range(S)]
 
     def z_step(k, h):
         def one(o, side):
@@ -249,38 +265,31 @@
             with jax.named_scope(f"y{k}"):
                 each_slice(k, one)
 
-    def finish_row(k):
+    def finish_row(k, parts):
         def one(o, side):
-            p_copy(o, s).start()
-            if square:
-                x_copy(o, nbr_x, 1, 0, nbr_x).wait_recv()
-                p_copy(o, nbr_x).start()
-                x_copy(o, nbr_y, 0, 0, nbr_y).wait_recv()
-                p_copy(o, nbr_y).start()
-                x_copy(o, diag, 0, 0, diag).wait_recv()
-                x_copy(o, diag, 1, 0, diag).wait_recv()
-                p_copy(o, diag).start()
-            else:
-                for j in range(1, S):
-                    p = lax.rem(s + S - j, S)
+            for i in parts:
+                p = order[i]
+                if i > 0 and square:
+                    for h in ((1,), (0,), (0, 1))[i - 1]:
+                        x_copy(o, p, h, 0, p).wait_recv()
+                elif i > 0:
                     for h in range(H):
-                        x_copy(o, p, h, j - 1, p).wait_recv()
-                    p_copy(o, p).start()
-
-        with jax.named_scope(f"fin{k}"):
+                        x_copy(o, p, h, i - 1, p).wait_recv()
+                p_copy(o, p).start()
+
+        with jax.named_scope(f"fin{k}{parts[0]}"):
             each_slice(k, one)
 
-    loads[0].wait()
-    loads[1].wait()
+    for c in loads[1:4]:
+        c.wait()
     tail = pl.ds(tokens - HALO, HALO)
     last_reach = jnp.max(least_tap[tokens - 1 : tokens, :], axis=1, keepdims=True)
     row_at = lax.broadcasted_iota(jnp.int32, (HALO, width), 0).astype(F32)
     newer = row_at >= last_reach + (HALO - n_taps)
     rim = jnp.where(newer, gate(value[tail, :], gates[tail, :]).astype(F32), jnp.float32(0.0))
     rim_out[0:HALO, :] = rim.astype(BF16)
-    rim_out[HALO : HALO + 16, :] = jnp.full(
-        (16, width), ids_ref[tokens - 1].astype(F32), F32
-    ).astype(BF16)
+    last_id = ids_row_ref[0:1, tokens - 1 : tokens].astype(F32)
+    rim_out[HALO : HALO + 16, :] = jnp.broadcast_to(last_id, (16, width)).astype(BF16)
     rim_copy = remote(
         rim_out, rim_in, rim_sem.at[0], rim_sem.at[1], lax.rem(s + 1, S), t
     )
@@ -335,12 +344,14 @@
             conv_out.at[to], conv_in.at[t], a2a_send.at[to], a2a_recv.at[t], s, to
         )
 
-    def conv_flush():
-        conv_copy(partner).start()
+    def conv_flush(inner):
+        if not inner:
+            conv_copy(partner).start()
         for far in range(1, Z):
             for to, there, _ in sides(far):
-
-                @pl.when(there)
+                middle = (to > 0) & (to < Z - 1)
+
+                @pl.when(there & (middle if inner else jnp.logical_not(middle)))
                 def _():
                     for c in range(2):
                         conv_copy(2 * to + c).start()
@@ -352,19 +363,22 @@
     z_step(1, 1)
     conv_some(marks[1], marks[2])
     z_step(2, 0)
-    x_step(1)
+    conv_flush(True)
     with jax.named_scope("rimwait"):
         rim_copy.wait()
-    same = (rim_in[HALO : HALO + 1, :].astype(F32) == ids_ref[0].astype(F32)) & (s > 0)
+    same = (rim_in[HALO : HALO + 1, :].astype(F32) == ids_row_ref[0:1, 0:1].astype(F32)) & (s > 0)
     padded[0:HALO, :] = jnp.where(same, rim_in[0:HALO, :].astype(F32), jnp.float32(0.0))
     conv_some(0, 1)
+    x_step(1)
     z_step(2, 1)
-    conv_flush()
+    conv_flush(False)
     y_step(1)
     conv_in[t, :, :] = conv_out[t, :, :]
 
     rows = block
     E = S
+    for c in loads[4:7]:
+        c.wait()
     cap = 2 * rows // E
     lane = lax.broadcasted_iota(jnp.int32, (rows, 128), 1)
     eye = lax.broadcasted_iota(jnp.int32, (rows, rows), 0) == lax.broadcasted_iota(
@@ -404,18 +418,21 @@
     for e in range(E):
         picks[e, :, :] = (slot_r[e : e + 1, :] == cap_i).astype(F32).astype(BF16)
 
+    all_parts = tuple(range(S))
     for k in range(3, Z):
         z_step(k, 0)
         x_step(k - 1)
         z_step(k, 1)
-        finish_row(k - 2)
+        finish_row(k - 2, all_parts)
         y_step(k - 1)
-    finish_row(Z - 2)
+    finish_row(Z - 1, all_parts[:1])
+    finish_row(Z - 2, all_parts[:-1])
     x_step(Z - 1)
     y_step(Z - 1)
-
-    total = jnp.zeros((rows, 1), F32)
+    finish_row(Z - 1, all_parts[1:-1])
+
     with jax.named_scope("a2await"):
+        total = jnp.sum(conv_in[t].astype(F32), axis=1, keepdims=True)
         for k in range(1, T):
             source = lax.rem(t + k, T)
             remote(
@@ -426,9 +443,8 @@
                 s,
                 source,
             ).wait_recv()
+            total = total + jnp.sum(conv_in[source].astype(F32), axis=1, keepdims=True)
     with jax.named_scope("act"):
-        for j in range(T):
-            total = total + jnp.sum(conv_in[j].astype(F32), axis=1, keepdims=True)
         average = total / (T * width)
         total = jnp.zeros((rows, 1), F32)
         for j in range(T):
@@ -442,14 +458,9 @@
             ] + bias_conv_ref[:, cols]
             act[:, cols] = (v / (1.0 + jnp.exp(-v))).astype(BF16)
 
-    finish_row(Z - 1)
-    loads[2].wait()
-    with jax.named_scope("wpwait"):
-        for o in range(Z):
-            for j in range(S):
-                p_wait(o, j)
-
-    others = [nbr_x, nbr_y, diag] if square else [lax.rem(s + S - k, S) for k in range(1, S)]
+    loads[7].wait()
+
+    others = order[1:]
     prompt = others[:2] if square else others
     late = others[2:] if square else []
 
@@ -497,6 +508,9 @@
         return pl.ds(pl.multiple_of(j * piece, piece), piece)
 
     def project(j, squares):
+        with jax.named_scope("wpwait"):
+            for o in range(Z):
+                p_wait(o, j)
         cols = piece_cols(j)
         acc = residual[:, cols].astype(F32)
         part = jnp.dot(act[...], wfull[j], preferred_element_type=F32)
@@ -512,13 +526,25 @@
         state = state.astype(F32)
         return squares + jnp.sum(state * state, axis=1, keepdims=True)
 
-    with jax.named_scope("project"):
-        squares = lax.fori_loop(0, S, project, jnp.zeros((rows, 1), F32))
-        for expert in late:
-            for j in range(S):
-                disp_copy(expert, j).start()
-
-    for c in loads[3:]:
+    def finish_last():
+        for k in (Z - 2, Z - 1):
+            finish_row(k, all_parts[-1:])
+
+    squares = jnp.zeros((rows, 1), F32)
+    if square:
+        for i, j in enumerate(order):
+            with jax.named_scope(f"project{i}"):
+                squares = project(j, squares)
+            if i == 0:
+                finish_last()
+    else:
+        finish_last()
+        squares = lax.fori_loop(0, S, project, squares)
+    for expert in late:
+        for j in order:
+            disp_copy(expert, j).start()
+
+    for c in loads[8:]:
         c.wait()
     ff = gate_w.shape[2]
     ff_step = min(ff, 256)
@@ -608,8 +634,7 @@
         acc = hidden[:, cols].astype(F32)
         for e in range(E):
             acc = acc + jnp.dot(spreads[e], returned[e, j], preferred_element_type=F32)
-        hidden[:, cols] = acc.astype(BF16)
-        pltpu.make_async_copy(hidden.at[:, cols], out_ref.at[:, cols], out_sem.at[j]).start()
+        out_ref[:, cols] = acc.astype(BF16)
         return 0
 
     with jax.named_scope("combine"):
@@ -649,9 +674,6 @@
             for j in range(S):
                 disp_copy(expert, j).wait_send()
                 ret_copy(expert, j).wait_send()
-        for j in range(S):
-            cols = piece_cols(j)
-            pltpu.make_async_copy(hidden.at[:, cols], out_ref.at[:, cols], out_sem.at[j]).wait()
 
 
 def body(
@@ -680,21 +702,24 @@
     G = group_router.shape[1]
     E = expert_router.shape[1]
     cap = 2 * rows // E
-    vmem = pl.BlockSpec(memory_space=pltpu.VMEM)
     hbm = pl.BlockSpec(memory_space=pl.ANY)
-    smem = pl.BlockSpec(memory_space=pltpu.SMEM)
     dma = pltpu.SemaphoreType.DMA
     piece = D // S
     Z = T // 2
     return pl.pallas_call(
         functools.partial(kernel, S, T, G),
-        out_shape=jax.ShapeDtypeStruct((rows, D), BF16),
-        in_specs=[
-            hbm, hbm, vmem, smem, vmem, vmem, vmem, hbm, hbm, vmem, vmem, vmem, vmem,
-            hbm, hbm, hbm,
-        ],
-        out_specs=hbm,
+        out_shape=pltpu.VMEM((rows, D), BF16),
+        in_specs=[hbm] * 15,
+        out_specs=pl.BlockSpec(memory_space=pltpu.VMEM),
         scratch_shapes=[
+            pltpu.VMEM((1, tokens), jnp.int32),
+            pltpu.VMEM(conv_kernel.shape, BF16),
+            pltpu.VMEM((1, T * width), F32),
+            pltpu.VMEM((1, T * width), F32),
+            pltpu.VMEM((1, D), F32),
+            pltpu.VMEM((G, D), BF16),
+            pltpu.VMEM((E, D), BF16),
+            pltpu.VMEM((2, rows), jnp.int32),
             pltpu.VMEM((tokens, width), BF16),
             pltpu.VMEM((tokens, width), BF16),
             pltpu.VMEM((S, T * wrows, piece), BF16),
@@ -720,7 +745,7 @@
             pltpu.VMEM((cap, ff), BF16),
             pltpu.VMEM((E, S, cap, piece), BF16),
             pltpu.VMEM((E, S, cap, piece), BF16),
-            dma((6,)),
+            dma((14,)),
             dma((S,)),
             dma((2,)),
             dma((2, Z, 2)),
@@ -735,7 +760,6 @@
             dma((S, S)),
             dma((S, S)),
             dma((S, S)),
-            dma((S,)),
         ],
         compiler_params=pltpu.CompilerParams(
             collective_id=0, has_side_effects=True, vmem_limit_bytes=60 * 1024 * 1024
@@ -744,7 +768,6 @@
         conv_value,
         conv_gate,
         doc_ids[None, :],
-        doc_ids,
         conv_kernel,
         norm_gain_conv[None, :],
         norm_bias_conv[None, :],

time: 85.6 us -> 79.6 us (0.930)
  Pallas kernels: 82 us -> 77.2 us
  local copies, waits for them, and re-layouts: 3.38 us -> 2.18 us
    pallas_call x1, Pallas kernels: 82 us -> 77.2 us  [body(): pl.pallas_call(functools.partial(kernel, S, T, G), out_shape=pltpu.VMEM((...]
    unnamed x1, local copies, waits for them, and re-layouts: 2.09 us -> 0.88 us
where the time goes in v3:
time: 79.6 us; the launch traced here: 79.4 us
  Pallas kernels  77.2 us (97%)
  local copies, waits for them, and re-layouts  2.18 us (3%)
    pallas_call x1, Pallas kernels, body(): pl.pallas_call(functools.partial(kernel, S, T, G), out_shape=pltpu.VMEM((...  77.2 us

profile of v3, /device:TPU:0, one launch (start us, length us, event | category | flops | bytes accessed | tf_op | source)
XLA Modules:
  0.0 79.4 jit_solution(4308768135161195969)
XLA Ops:
  0.0 1.3 %broadcast_in_dim.12.ids_hbm = s32[1,1536]{1,0:T(1,128)} reshape(s32[1536]{0:T(1024)} %param.17) | data formatting | bytes 12288 | tf_op jit(solution)/shard_map/broadcast_in_dim | solution.py:770
  1.3 77.2 %shard_map.145 = bf16[192,2048]{1,0:T(8,128)(2,1)S(1)} custom-call(bf16[1536,256]{1,0:T(8,128)(2,1)} %value_hbm.1, bf16[1536,256]{1,0:T(8,128)(2,1)} %gate_hbm.1, s32[1,1536]{1,0:T(1,128)} %broadcast_in_dim.12.ids_hbm, bf16[31,256]{1,0:T(8,128)(2,1)} %kernel_hbm.1, f32[1,2048]{1,0:T(1,128)} %bitcast.7, f32[1,2048]{1,0:T(1,128)} %bitcast.8, ...), custom_call_target="tpu_custom_call" | custom-call | tf_op jit(solution)/shard_map/pallas_call | solution.py:709
  78.5 0.9 %copy.17 = bf16[192,2048]{1,0:T(8,128)(2,1)} copy(bf16[192,2048]{1,0:T(8,128)(2,1)S(1)} %shard_map.145) | data formatting | bytes 1572864

commit v4 on v3

--- a/solution.py
+++ b/solution.py
@@ -12,6 +12,7 @@
 F32 = jnp.float32
 BF16 = jnp.bfloat16
 HALO = 32
+CHUNKS = 2
 
 
 def gate(value, gate_value):
@@ -71,6 +72,14 @@
     ffn_hidden,
     results,
     returned,
+    router_all,
+    down_stage,
+    down_x,
+    h_own,
+    h_out,
+    h_in,
+    back_out,
+    back_in,
     local_sem,
     wl_sem,
     rim_sem,
@@ -86,6 +95,17 @@
     disp_recv,
     ret_send,
     ret_recv,
+    ex_send,
+    ex_recv,
+    hx_send,
+    hx_recv,
+    rt_send,
+    rt_recv,
+    zd_send,
+    zd_recv,
+    dp_send,
+    dp_recv,
+    dx_sem,
 ):
     s = lax.axis_index("sp")
     t = lax.axis_index("tp")
@@ -100,6 +120,9 @@
     wrows = wfull.shape[1] // T
     D = S * piece
     square = S == 4
+    E = S
+    paired = square and E == 2 * G
+    wide = D // T
     H = 2
     part_rows = wrows // H
 
@@ -151,9 +174,16 @@
         )
         for j in range(S)
     ]
+    stage = pltpu.make_async_copy(
+        down_w_hbm.at[0, :, pl.ds(pl.multiple_of(t * wide, wide), wide)],
+        down_stage,
+        local_sem.at[14],
+    )
     loads[0].start()
     for c in own_w:
         c.start()
+    if paired:
+        stage.start()
     for c in loads[1:]:
         c.start()
 
@@ -215,6 +245,12 @@
 
     for j in range(S):
         p_copy(z, j).start()
+    dx_copy = remote(
+        down_stage, down_x.at[t], dx_sem.at[0], dx_sem.at[1], s + 1 - 2 * (s % 2), t
+    )
+    if paired:
+        stage.wait()
+        dx_copy.start()
 
     def sides(k):
         return ((z - k, z - k >= 0, 0), (z + k, z + k < Z, 1))
@@ -264,6 +300,44 @@
         if square:
             with jax.named_scope(f"y{k}"):
                 each_slice(k, one)
+
+    def zd_copy(o, side, to):
+        ref = down_x.at[2 * o + core]
+        return remote(ref, ref, zd_send.at[side, o], zd_recv.at[o], s, 2 * to + core)
+
+    def dp_copy(o):
+        ref = down_x.at[2 * o + core]
+        return remote(ref, ref, dp_send.at[o], dp_recv.at[o], s, partner)
+
+    def dp_wait(o):
+        ref = down_x.at[2 * o + 1 - core]
+        remote(ref, ref, dp_send.at[o], dp_recv.at[o], s, partner).wait_recv()
+
+    def d_start():
+        dx_copy.wait_recv()
+
+        @pl.when(has_up)
+        def _():
+            zd_copy(z, 0, z + 1).start()
+
+        @pl.when(has_down)
+        def _():
+            zd_copy(z, 1, z - 1).start()
+
+        dp_copy(z).start()
+
+    def d_step(k):
+        def one(o, side):
+            zd_copy(o, side, z).wait_recv()
+
+            @pl.when(has_down if side else has_up)
+            def _():
+                zd_copy(o, side, z - 1 if side else z + 1).start()
+
+            dp_copy(o).start()
+
+        with jax.named_scope(f"d{k}"):
+            each_slice(k, one)
 
     def finish_row(k, parts):
         def one(o, side):
@@ -376,7 +450,6 @@
     conv_in[t, :, :] = conv_out[t, :, :]
 
     rows = block
-    E = S
     for c in loads[4:7]:
         c.wait()
     cap = 2 * rows // E
@@ -444,6 +517,9 @@
                 source,
             ).wait_recv()
             total = total + jnp.sum(conv_in[source].astype(F32), axis=1, keepdims=True)
+    if paired:
+        with jax.named_scope("d0"):
+            d_start()
     with jax.named_scope("act"):
         average = total / (T * width)
         total = jnp.zeros((rows, 1), F32)
@@ -464,181 +540,467 @@
     prompt = others[:2] if square else others
     late = others[2:] if square else []
 
-    def disp_copy(expert, j):
-        return remote(
-            outgoing.at[expert, j],
-            arrived.at[s, j],
-            disp_send.at[expert, j],
-            disp_recv.at[s, j],
-            expert,
-            t,
-        )
-
-    def disp_wait(sender, j):
-        remote(
-            outgoing.at[sender, j],
-            arrived.at[sender, j],
-            disp_send.at[sender, j],
-            disp_recv.at[sender, j],
-            sender,
-            t,
-        ).wait_recv()
-
-    def ret_copy(sender, j):
-        return remote(
-            results.at[sender, j],
-            returned.at[s, j],
-            ret_send.at[sender, j],
-            ret_recv.at[s, j],
-            sender,
-            t,
-        )
-
-    def ret_wait(expert, j):
-        remote(
-            results.at[expert, j],
-            returned.at[expert, j],
-            ret_send.at[expert, j],
-            ret_recv.at[expert, j],
-            expert,
-            t,
-        ).wait_recv()
-
     def piece_cols(j):
         return pl.ds(pl.multiple_of(j * piece, piece), piece)
-
-    def project(j, squares):
-        with jax.named_scope("wpwait"):
-            for o in range(Z):
-                p_wait(o, j)
-        cols = piece_cols(j)
-        acc = residual[:, cols].astype(F32)
-        part = jnp.dot(act[...], wfull[j], preferred_element_type=F32)
-        state = (acc + part).astype(BF16)
-        hidden[:, cols] = state
-        for expert in others:
-            outgoing[expert, j, :, :] = jnp.dot(
-                picks[expert], state, preferred_element_type=F32
-            ).astype(BF16)
-        for expert in prompt:
-            disp_copy(expert, j).start()
-        arrived[s, j, :, :] = jnp.dot(picks[s], state, preferred_element_type=F32).astype(BF16)
-        state = state.astype(F32)
-        return squares + jnp.sum(state * state, axis=1, keepdims=True)
 
     def finish_last():
         for k in (Z - 2, Z - 1):
             finish_row(k, all_parts[-1:])
 
-    squares = jnp.zeros((rows, 1), F32)
-    if square:
-        for i, j in enumerate(order):
-            with jax.named_scope(f"project{i}"):
-                squares = project(j, squares)
-            if i == 0:
-                finish_last()
-    else:
-        finish_last()
-        squares = lax.fori_loop(0, S, project, squares)
-    for expert in late:
-        for j in order:
-            disp_copy(expert, j).start()
-
-    for c in loads[8:]:
-        c.wait()
-    ff = gate_w.shape[2]
-    ff_step = min(ff, 256)
-
-    def expert_block(sender, target, send):
-        def square_step(j, squares):
-            x = arrived[sender, j].astype(F32)
-            return squares + jnp.sum(x * x, axis=1, keepdims=True)
-
-        total = lax.fori_loop(0, S, square_step, jnp.zeros((cap, 1), F32))
-        row_scale = lax.rsqrt(total / D + epsilon)
-
-        def norm_step(j, _):
-            cols = piece_cols(j)
-            x = arrived[sender, j].astype(F32)
-            normed_in[:, cols] = (x * row_scale * gain_moe_ref[:, cols]).astype(BF16)
-            return 0
-
-        lax.fori_loop(0, S, norm_step, 0)
-
-        def up_step(j, _):
-            cols = pl.ds(pl.multiple_of(j * ff_step, ff_step), ff_step)
-            x = normed_in[...]
-            g = jnp.dot(x, gate_w[0, :, cols], preferred_element_type=F32)
-            u = jnp.dot(x, up_w[0, :, cols], preferred_element_type=F32)
-            ffn_hidden[:, cols] = (g / (1.0 + jnp.exp(-g)) * u).astype(BF16)
-            return 0
-
-        lax.fori_loop(0, ff // ff_step, up_step, 0)
-
-        def down_step(j, _):
-            target[j, :, :] = jnp.dot(
-                ffn_hidden[...], down_w[0, :, piece_cols(j)], preferred_element_type=F32
-            ).astype(BF16)
-            if send:
-                ret_copy(sender, j).start()
-            return 0
-
-        lax.fori_loop(0, S, down_step, 0)
-
-    with jax.named_scope("ffnown"):
-        expert_block(s, returned.at[s], False)
-
-    scale = lax.rsqrt(squares / D + epsilon)
-
-    def norm_cols(j, _):
-        cols = piece_cols(j)
-        normed[:, cols] = (hidden[:, cols].astype(F32) * scale * gain_moe_ref[:, cols]).astype(BF16)
-        return 0
-
-    def logits(router):
-        return lax.dot_general(
-            normed[...], router[...], (((1,), (1,)), ((), ())), preferred_element_type=F32
-        )
-
     def column(array, expert):
         mine = lane[:, : array.shape[1]] == expert
         return jnp.sum(jnp.where(mine, array, jnp.float32(0.0)), axis=1, keepdims=True)
 
     zero = jnp.float32(0.0)
-    with jax.named_scope("router"):
-        lax.fori_loop(0, S, norm_cols, 0)
-        group_exp = jnp.exp(logits(group_router_ref))
-        expert_exp = jnp.exp(logits(expert_router_ref))
-        group_prob = jnp.sum(
-            jnp.where(in_group[:, :G], group_exp, zero), axis=1, keepdims=True
-        ) / jnp.sum(group_exp, axis=1, keepdims=True)
-        chosen_exp = jnp.where(chosen[:, :E], expert_exp, zero)
-        mix = group_prob * chosen_exp / jnp.sum(chosen_exp, axis=1, keepdims=True)
-        slot_iota = lax.broadcasted_iota(jnp.int32, (rows, cap), 1).astype(F32)
-        for e in range(E):
+    slot_iota = lax.broadcasted_iota(jnp.int32, (rows, cap), 1).astype(F32)
+    ff = gate_w.shape[2]
+    ff_step = min(ff, 256)
+
+
+    if paired:
+        C = CHUNKS
+        part = cap // C
+        mates = (s, nbr_x)
+
+        def chunk(c):
+            return pl.ds(c * part, part)
+
+        def a_copy(j):
+            return remote(
+                outgoing.at[0, j], arrived.at[0, j], ex_send.at[0, j], ex_recv.at[0, j], nbr_x, t
+            )
+
+        def b_copy(j, c):
+            return remote(
+                outgoing.at[1, j, chunk(c), :],
+                arrived.at[1, j, chunk(c), :],
+                ex_send.at[1 + c, j],
+                ex_recv.at[1 + c, j],
+                nbr_y,
+                t,
+            )
+
+        def f_copy(j, c):
+            return remote(
+                arrived.at[1, j, chunk(c), :],
+                arrived.at[2, j, chunk(c), :],
+                ex_send.at[1 + C + c, j],
+                ex_recv.at[1 + C + c, j],
+                nbr_x,
+                t,
+            )
+
+        def h_rows(kind, c):
+            return pl.ds(0, cap) if kind == 0 else chunk(c)
+
+        def hx_copy(kind, c):
+            at = h_rows(kind, c)
+            return remote(
+                h_out.at[kind, at, :],
+                h_in.at[kind, at, :],
+                hx_send.at[kind, c],
+                hx_recv.at[kind, c],
+                nbr_x,
+                t,
+            )
+
+        def rt_copy(q, c):
+            return remote(
+                back_out.at[q, chunk(c), :],
+                back_in.at[q, chunk(c), :],
+                rt_send.at[q, c],
+                rt_recv.at[q, c],
+                nbr_y,
+                t,
+            )
+
+        y_order = [nbr_y, diag, s, nbr_x]
+
+        def project(i, j):
+            with jax.named_scope("wpwait"):
+                for o in range(Z):
+                    p_wait(o, j)
+            cols = piece_cols(j)
+            acc = residual[:, cols].astype(F32)
+            acc = acc + jnp.dot(act[...], wfull[j], preferred_element_type=F32)
+            state = acc.astype(BF16)
+            hidden[:, cols] = state
+            outgoing[1, j, :, :] = jnp.dot(
+                picks[nbr_y], state, preferred_element_type=F32
+            ).astype(BF16)
+            b_copy(j, 0).start()
+            outgoing[0, j, :, :] = jnp.dot(
+                picks[s], state, preferred_element_type=F32
+            ).astype(BF16)
+            if i < 2:
+                a_copy(j).start()
+
+        def forward(c, first, last):
+            with jax.named_scope(f"fwd{c}{first}"):
+                for j in y_order[first:last]:
+                    b_copy(j, c).wait_recv()
+                    f_copy(j, c).start()
+
+        router_lane = lax.broadcasted_iota(jnp.int32, (1, router_all.shape[0]), 1)
+        group_lane = router_lane < G
+        own_group_lane = router_lane == s // 2
+        own_lane = router_lane == s + G
+        mate_lane = (router_lane == s + G) | (router_lane == nbr_x + G)
+
+        def gate_up(source, at, count, target):
+            def square_step(j, squares):
+                x = source[j, at, :].astype(F32)
+                return squares + jnp.sum(x * x, axis=1, keepdims=True)
+
+            total = lax.fori_loop(0, S, square_step, jnp.zeros((count, 1), F32))
+            row_scale = lax.rsqrt(total / D + epsilon)
+
+            def norm_step(j, _):
+                cols = piece_cols(j)
+                x = source[j, at, :].astype(F32)
+                normed_in[0:count, cols] = (x * row_scale * gain_moe_ref[:, cols]).astype(BF16)
+                return 0
+
+            lax.fori_loop(0, S, norm_step, 0)
+            logits = lax.dot_general(
+                normed_in[0:count, :],
+                router_all[...],
+                (((1,), (1,)), ((), ())),
+                preferred_element_type=F32,
+            )
+            exps = jnp.exp(logits)
+
+            def over(mask):
+                return jnp.sum(jnp.where(mask, exps, zero), axis=1, keepdims=True)
+
+            weight = over(own_group_lane) / over(group_lane) * over(own_lane) / over(mate_lane)
+
+            def up_step(j, _):
+                cols = pl.ds(pl.multiple_of(j * ff_step, ff_step), ff_step)
+                x = normed_in[0:count, :]
+                g = jnp.dot(x, gate_w[0, :, cols], preferred_element_type=F32)
+                u = jnp.dot(x, up_w[0, :, cols], preferred_element_type=F32)
+                target[at, cols] = (g / (1.0 + jnp.exp(-g)) * u * weight).astype(BF16)
+                return 0
+
+            lax.fori_loop(0, ff // ff_step, up_step, 0)
+
+        def each_block(k, act_on):
+            def pair(o, side):
+                def one(c2, _):
+                    act_on(2 * o + c2)
+                    return 0
+
+                lax.fori_loop(0, 2, one, 0)
+
+            if k == 0:
+                pair(z, 0)
+            else:
+                each_slice(k, pair)
+
+        def wide_cols(q):
+            return pl.ds(pl.multiple_of(q * wide, wide), wide)
+
+        def both(kind, at, q):
+            acc = jnp.dot(
+                h_own[kind, at, :], down_w[0, :, wide_cols(q)], preferred_element_type=F32
+            )
+            acc = acc + jnp.dot(h_in[kind, at, :], down_x[q], preferred_element_type=F32)
+            return acc.astype(BF16)
+
+        def down_b(k, c):
+            def block_of(q):
+                back_out[q, chunk(c), :] = both(1, chunk(c), q)
+                rt_copy(q, c).start()
+
+            with jax.named_scope(f"down{k}{c}"):
+                if c == 0:
+                    if k == 0:
+                        dp_wait(z)
+                    else:
+                        each_slice(k, lambda o, side: dp_wait(o))
+                each_block(k, block_of)
+
+        for i, j in enumerate(order):
+            with jax.named_scope(f"project{i}"):
+                project(i, j)
+            if i == 0:
+                finish_last()
+        for c in range(1, C):
+            for j in order:
+                b_copy(j, c).start()
+        forward(0, 0, S // 2)
+        for c in loads[8:]:
+            c.wait()
+        blank = jnp.zeros((router_all.shape[0] - G - E, D), F32)
+        router_all[...] = jnp.concatenate(
+            [group_router_ref[...].astype(F32), expert_router_ref[...].astype(F32), blank], axis=0
+        ).astype(BF16)
+        forward(0, S // 2, S)
+        everyone = pl.ds(0, cap)
+        with jax.named_scope("guB0"):
+            gate_up(arrived.at[1], chunk(0), part, h_own.at[1])
+        forward(1, 0, S // 2)
+        with jax.named_scope("guA"):
+            gate_up(outgoing.at[0], everyone, cap, h_own.at[0])
+        forward(1, S // 2, S)
+        d_step(1)
+        with jax.named_scope("fw0"):
+            for j in y_order:
+                f_copy(j, 0).wait_recv()
+        with jax.named_scope("guF0"):
+            gate_up(arrived.at[2], chunk(0), part, h_out.at[1])
+        hx_copy(1, 0).start()
+        a_copy(order[2]).start()
+        with jax.named_scope("guB1"):
+            gate_up(arrived.at[1], chunk(1), part, h_own.at[1])
+        with jax.named_scope("fw1"):
+            for j in y_order:
+                f_copy(j, 1).wait_recv()
+        with jax.named_scope("guF1"):
+            gate_up(arrived.at[2], chunk(1), part, h_out.at[1])
+        hx_copy(1, 1).start()
+        a_copy(order[3]).start()
+        d_step(2)
+        for e, at in enumerate((s, nbr_y)):
             spreads[e, :, :] = jnp.where(
-                column(slot, e) == slot_iota, column(mix, e), zero
+                column(slot, at) == slot_iota, jnp.float32(1.0), zero
             ).astype(BF16)
-
-    for i, sender in enumerate(others):
-        with jax.named_scope(f"dispwait{i}"):
+        with jax.named_scope("hw0"):
+            hx_copy(1, 0).wait_recv()
+        down_b(0, 0)
+        down_b(1, 0)
+        with jax.named_scope("hw1"):
+            hx_copy(1, 1).wait_recv()
+        down_b(0, 1)
+        down_b(1, 1)
+        with jax.named_scope("aw"):
+            for j in order:
+                a_copy(j).wait_recv()
+        with jax.named_scope("guX"):
+            gate_up(arrived.at[0], everyone, cap, h_out.at[0])
+        hx_copy(0, 0).start()
+        for k in range(2, Z):
+            if k > 2:
+                d_step(k)
+            for c in range(C):
+                down_b(k, c)
+        with jax.named_scope("hwA"):
+            hx_copy(0, 0).wait_recv()
+
+        def combine(q):
+            for c in range(C):
+                rt_copy(q, c).wait_recv()
+            cols = wide_cols(q)
+            acc = hidden[:, cols].astype(F32)
+            acc = acc + jnp.dot(spreads[0], both(0, everyone, q), preferred_element_type=F32)
+            acc = acc + jnp.dot(spreads[1], back_in[q], preferred_element_type=F32)
+            out_ref[:, cols] = acc.astype(BF16)
+
+        for k in range(Z):
+            with jax.named_scope(f"combine{k}"):
+                each_block(k, combine)
+
+        with jax.named_scope("sendwait"):
+            dx_copy.wait_send()
+            for i in range(S):
+                a_copy(i).wait_send()
+                for c in range(C):
+                    b_copy(i, c).wait_send()
+                    f_copy(i, c).wait_send()
+            hx_copy(0, 0).wait_send()
+            for c in range(C):
+                hx_copy(1, c).wait_send()
+                for q in range(T):
+                    rt_copy(q, c).wait_send()
+
+            @pl.when(has_up)
+            def _():
+                zd_copy(z, 0, z + 1).wait_send()
+
+            @pl.when(has_down)
+            def _():
+                zd_copy(z, 1, z - 1).wait_send()
+
+            dp_copy(z).wait_send()
+
+            def d_sent(o, side):
+                @pl.when(has_down if side else has_up)
+                def _():
+                    zd_copy(o, side, z - 1 if side else z + 1).wait_send()
+
+                dp_copy(o).wait_send()
+
+            for k in range(1, Z):
+                each_slice(k, d_sent)
+
+    else:
+        def disp_copy(expert, j):
+            return remote(
+                outgoing.at[expert, j],
+                arrived.at[s, j],
+                disp_send.at[expert, j],
+                disp_recv.at[s, j],
+                expert,
+                t,
+            )
+
+        def disp_wait(sender, j):
+            remote(
+                outgoing.at[sender, j],
+                arrived.at[sender, j],
+                disp_send.at[sender, j],
+                disp_recv.at[sender, j],
+                sender,
+                t,
+            ).wait_recv()
+
+        def ret_copy(sender, j):
+            return remote(
+                results.at[sender, j],
+                returned.at[s, j],
+                ret_send.at[sender, j],
+                ret_recv.at[s, j],
+                sender,
+                t,
+            )
+
+        def ret_wait(expert, j):
+            remote(
+                results.at[expert, j],
+                returned.at[expert, j],
+                ret_send.at[expert, j],
+                ret_recv.at[expert, j],
+                expert,
+                t,
+            ).wait_recv()
+
+        def project(j, squares):
+            with jax.named_scope("wpwait"):
+                for o in range(Z):
+                    p_wait(o, j)
+            cols = piece_cols(j)
+            acc = residual[:, cols].astype(F32)
+            part = jnp.dot(act[...], wfull[j], preferred_element_type=F32)
+            state = (acc + part).astype(BF16)
+            hidden[:, cols] = state
+            for expert in others:
+                outgoing[expert, j, :, :] = jnp.dot(
+                    picks[expert], state, preferred_element_type=F32
+                ).astype(BF16)
+            for expert in prompt:
+                disp_copy(expert, j).start()
+            arrived[s, j, :, :] = jnp.dot(picks[s], state, preferred_element_type=F32).astype(BF16)
+            state = state.astype(F32)
+            return squares + jnp.sum(state * state, axis=1, keepdims=True)
+
+        squares = jnp.zeros((rows, 1), F32)
+        if square:
+            for i, j in enumerate(order):
+                with jax.named_scope(f"project{i}"):
+                    squares = project(j, squares)
+                if i == 0:
+                    finish_last()
+        else:
+            finish_last()
+            squares = lax.fori_loop(0, S, project, squares)
+        for expert in late:
+            for j in order:
+                disp_copy(expert, j).start()
+
+        for c in loads[8:]:
+            c.wait()
+
+        def expert_block(sender, target, send):
+            def square_step(j, squares):
+                x = arrived[sender, j].astype(F32)
+                return squares + jnp.sum(x * x, axis=1, keepdims=True)
+
+            total = lax.fori_loop(0, S, square_step, jnp.zeros((cap, 1), F32))
+            row_scale = lax.rsqrt(total / D + epsilon)
+
+            def norm_step(j, _):
+                cols = piece_cols(j)
+                x = arrived[sender, j].astype(F32)
+                normed_in[:, cols] = (x * row_scale * gain_moe_ref[:, cols]).astype(BF16)
+                return 0
+
+            lax.fori_loop(0, S, norm_step, 0)
+
+            def up_step(j, _):
+                cols = pl.ds(pl.multiple_of(j * ff_step, ff_step), ff_step)
+                x = normed_in[...]
+                g = jnp.dot(x, gate_w[0, :, cols], preferred_element_type=F32)
+                u = jnp.dot(x, up_w[0, :, cols], preferred_element_type=F32)
+                ffn_hidden[:, cols] = (g / (1.0 + jnp.exp(-g)) * u).astype(BF16)
+                return 0
+
+            lax.fori_loop(0, ff // ff_step, up_step, 0)
+
+            def down_step(j, _):
+                target[j, :, :] = jnp.dot(
+                    ffn_hidden[...], down_w[0, :, piece_cols(j)], preferred_element_type=F32
+                ).astype(BF16)
+                if send:
+                    ret_copy(sender, j).start()
+                return 0
+
+            lax.fori_loop(0, S, down_step, 0)
+
+        with jax.named_scope("ffnown"):
+            expert_block(s, returned.at[s], False)
+
+        scale = lax.rsqrt(squares / D + epsilon)
+
+        def norm_cols(j, _):
+            cols = piece_cols(j)
+            normed[:, cols] = (hidden[:, cols].astype(F32) * scale * gain_moe_ref[:, cols]).astype(BF16)
+            return 0
+
+        def logits(router):
+            return lax.dot_general(
+                normed[...], router[...], (((1,), (1,)), ((), ())), preferred_element_type=F32
+            )
+
+        with jax.named_scope("router"):
+            lax.fori_loop(0, S, norm_cols, 0)
+            group_exp = jnp.exp(logits(group_router_ref))
+            expert_exp = jnp.exp(logits(expert_router_ref))
+            group_prob = jnp.sum(
+                jnp.where(in_group[:, :G], group_exp, zero), axis=1, keepdims=True
+            ) / jnp.sum(group_exp, axis=1, keepdims=True)
+            chosen_exp = jnp.where(chosen[:, :E], expert_exp, zero)
+            mix = group_prob * chosen_exp / jnp.sum(chosen_exp, axis=1, keepdims=True)
+            for e in range(E):
+                spreads[e, :, :] = jnp.where(
+                    column(slot, e) == slot_iota, column(mix, e), zero
+                ).astype(BF16)
+
+        for i, sender in enumerate(others):
+            with jax.named_scope(f"dispwait{i}"):
+                for j in range(S):
+                    disp_wait(sender, j)
+            with jax.named_scope(f"ffn{i}"):
+                expert_block(sender, results.at[sender], True)
+
+        def combine(j, _):
+            cols = piece_cols(j)
+            for expert in others:
+                ret_wait(expert, j)
+            acc = hidden[:, cols].astype(F32)
+            for e in range(E):
+                acc = acc + jnp.dot(spreads[e], returned[e, j], preferred_element_type=F32)
+            out_ref[:, cols] = acc.astype(BF16)
+            return 0
+
+        with jax.named_scope("combine"):
+            lax.fori_loop(0, S, combine, 0)
+
+
+        for expert in others:
             for j in range(S):
-                disp_wait(sender, j)
-        with jax.named_scope(f"ffn{i}"):
-            expert_block(sender, results.at[sender], True)
-
-    def combine(j, _):
-        cols = piece_cols(j)
-        for expert in others:
-            ret_wait(expert, j)
-        acc = hidden[:, cols].astype(F32)
-        for e in range(E):
-            acc = acc + jnp.dot(spreads[e], returned[e, j], preferred_element_type=F32)
-        out_ref[:, cols] = acc.astype(BF16)
-        return 0
-
-    with jax.named_scope("combine"):
-        lax.fori_loop(0, S, combine, 0)
+                disp_copy(expert, j).wait_send()
+                ret_copy(expert, j).wait_send()
 
     with jax.named_scope("sendwait"):
         for h in range(H):
@@ -670,10 +1032,6 @@
             each_slice(k, sent)
         for k in range(1, T):
             conv_copy(lax.rem(t + k, T)).wait_send()
-        for expert in others:
-            for j in range(S):
-                disp_copy(expert, j).wait_send()
-                ret_copy(expert, j).wait_send()
 
 
 def body(
@@ -745,7 +1103,15 @@
             pltpu.VMEM((cap, ff), BF16),
             pltpu.VMEM((E, S, cap, piece), BF16),
             pltpu.VMEM((E, S, cap, piece), BF16),
-            dma((14,)),
+            pltpu.VMEM((G + E + (-G - E) % 8, D), BF16),
+            pltpu.VMEM((ff, D // T), BF16),
+            pltpu.VMEM((T, ff, D // T), BF16),
+            pltpu.VMEM((2, cap, ff), BF16),
+            pltpu.VMEM((2, cap, ff), BF16),
+            pltpu.VMEM((2, cap, ff), BF16),
+            pltpu.VMEM((T, cap, D // T), BF16),
+            pltpu.VMEM((T, cap, D // T), BF16),
+            dma((15,)),
             dma((S,)),
             dma((2,)),
             dma((2, Z, 2)),
@@ -760,6 +1126,17 @@
             dma((S, S)),
             dma((S, S)),
             dma((S, S)),
+            dma((1 + 2 * CHUNKS, S)),
+            dma((1 + 2 * CHUNKS, S)),
+            dma((2, CHUNKS)),
+            dma((2, CHUNKS)),
+            dma((T, CHUNKS)),
+            dma((T, CHUNKS)),
+            dma((2, Z)),
+            dma((Z,)),
+            dma((Z,)),
+            dma((Z,)),
+            dma((2,)),
         ],
         compiler_params=pltpu.CompilerParams(
             collective_id=0, has_side_effects=True, vmem_limit_bytes=60 * 1024 * 1024

time: 79.6 us -> 75 us (0.942)
  Pallas kernels: 77.2 us -> 72.6 us
    pallas_call x1, Pallas kernels: 77.2 us -> 72.6 us  [body(): pl.pallas_call(functools.partial(kernel, S, T, G), out_shape=pltpu.VMEM((...]
where the time goes in v4:
time: 75 us; the launch traced here: 74.7 us
  Pallas kernels  72.6 us (97%)
  local copies, waits for them, and re-layouts  2.18 us (3%)
    pallas_call x1, Pallas kernels, body(): pl.pallas_call(functools.partial(kernel, S, T, G), out_shape=pltpu.VMEM((...  72.6 us

profile of v4, /device:TPU:0, one launch (start us, length us, event | category | flops | bytes accessed | tf_op | source)
XLA Modules:
  0.0 74.7 jit_solution(13091614918717698287)
XLA Ops:
  0.0 1.3 %broadcast_in_dim.12.ids_hbm = s32[1,1536]{1,0:T(1,128)} reshape(s32[1536]{0:T(1024)} %param.17) | data formatting | bytes 12288 | tf_op jit(solution)/shard_map/broadcast_in_dim | solution.py:1147
  1.3 72.6 %shard_map.145 = bf16[192,2048]{1,0:T(8,128)(2,1)S(1)} custom-call(bf16[1536,256]{1,0:T(8,128)(2,1)} %value_hbm.1, bf16[1536,256]{1,0:T(8,128)(2,1)} %gate_hbm.1, s32[1,1536]{1,0:T(1,128)} %broadcast_in_dim.12.ids_hbm, bf16[31,256]{1,0:T(8,128)(2,1)} %kernel_hbm.1, f32[1,2048]{1,0:T(1,128)} %bitcast.7, f32[1,2048]{1,0:T(1,128)} %bitcast.8, ...), custom_call_target="tpu_custom_call" | custom-call | tf_op jit(solution)/shard_map/pallas_call | solution.py:1067
  73.9 0.9 %copy.17 = bf16[192,2048]{1,0:T(8,128)(2,1)} copy(bf16[192,2048]{1,0:T(8,128)(2,1)S(1)} %shard_map.145) | data formatting | bytes 1572864

commit v5 on v4

--- a/solution.py
+++ b/solution.py
@@ -80,6 +80,9 @@
     h_in,
     back_out,
     back_in,
+    own_down,
+    spread_all,
+    base_out,
     local_sem,
     wl_sem,
     rim_sem,
@@ -121,7 +124,7 @@
     D = S * piece
     square = S == 4
     E = S
-    paired = square and E == 2 * G
+    paired = square and expert_router_ref.shape[0] == S and E == 2 * G
     wide = D // T
     H = 2
     part_rows = wrows // H
@@ -167,12 +170,18 @@
             ]
         )
     ]
+    nbr_x = s + 1 - 2 * (s % 2)
+    nbr_y = s + 2 - 4 * (s // 2)
+    diag = 3 - s
+    order = [s, nbr_x, nbr_y, diag] if square else [lax.rem(s + S - j, S) for j in range(S)]
     own_rows = pl.ds(pl.multiple_of(t * wrows, wrows), wrows)
     own_w = [
         pltpu.make_async_copy(
-            weight_hbm.at[:, pl.ds(j * piece, piece)], wfull.at[j, own_rows, :], wl_sem.at[j]
+            weight_hbm.at[:, pl.ds(pl.multiple_of(j * piece, piece), piece)],
+            wfull.at[j, own_rows, :],
+            wl_sem.at[i],
         )
-        for j in range(S)
+        for i, j in enumerate(order)
     ]
     stage = pltpu.make_async_copy(
         down_w_hbm.at[0, :, pl.ds(pl.multiple_of(t * wide, wide), wide)],
@@ -180,11 +189,10 @@
         local_sem.at[14],
     )
     loads[0].start()
-    for c in own_w:
-        c.start()
+    own_w[0].start()
     if paired:
         stage.start()
-    for c in loads[1:]:
+    for c in loads[1:4]:
         c.start()
 
     loads[0].wait()
@@ -215,24 +223,22 @@
         ref = w_ref(o, s, h)
         return remote(ref, ref, wz_send.at[up, o, h], wz_recv.at[o, h], s, 2 * to + core)
 
-    def x_copy(o, p, h, lane_at, to):
+    def x_copy(o, p, h, role, to):
         ref = w_ref(o, p, h)
-        return remote(ref, ref, wx_send.at[lane_at, o, h], wx_recv.at[p, o, h], to, t)
+        return remote(ref, ref, wx_send.at[0], wx_recv.at[role, o, h], to, t)
 
     def p_copy(o, p):
         rows_at = pl.ds(pl.multiple_of((2 * o + core) * wrows, wrows), wrows)
         ref = wfull.at[p, rows_at, :]
-        return remote(ref, ref, wp_send.at[o, p], wp_recv.at[o, p], s, partner)
-
-    def p_wait(o, p):
-        rows_at = pl.ds(pl.multiple_of((2 * o + 1 - core) * wrows, wrows), wrows)
-        ref = wfull.at[p, rows_at, :]
-        remote(ref, ref, wp_send.at[o, p], wp_recv.at[o, p], s, partner).wait_recv()
+        return remote(ref, ref, wp_send.at[0], wp_recv.at[p], s, partner)
+
+    def p_wait(p):
+        ref = wfull.at[p, pl.ds(0, Z * wrows), :]
+        remote(ref, ref, wp_send.at[0], wp_recv.at[p], s, partner).wait_recv()
 
     has_up = z + 1 < Z
     has_down = z > 0
-    for j in range(S):
-        own_w[j].wait()
+    own_w[0].wait()
     for h in range(H):
 
         @pl.when(has_up)
@@ -243,14 +249,15 @@
         def _():
             z_copy(z, h, 1, z - 1).start()
 
-    for j in range(S):
-        p_copy(z, j).start()
-    dx_copy = remote(
-        down_stage, down_x.at[t], dx_sem.at[0], dx_sem.at[1], s + 1 - 2 * (s % 2), t
-    )
+    for c in own_w[1:]:
+        c.start()
+    for c in loads[4:]:
+        c.start()
+    dx_copy = remote(down_stage, down_x.at[t], dx_sem.at[0], dx_sem.at[1], nbr_x, t)
     if paired:
         stage.wait()
         dx_copy.start()
+    p_copy(z, s).start()
 
     def sides(k):
         return ((z - k, z - k >= 0, 0), (z + k, z + k < Z, 1))
@@ -258,11 +265,6 @@
     def each_slice(k, act_on):
         for o, there, side in sides(k):
             pl.when(there)(functools.partial(act_on, o, side))
-
-    nbr_x = s + 1 - 2 * (s % 2)
-    nbr_y = s + 2 - 4 * (s // 2)
-    diag = 3 - s
-    order = [s, nbr_x, nbr_y, diag] if square else [lax.rem(s + S - j, S) for j in range(S)]
 
     def z_step(k, h):
         def one(o, side):
@@ -285,7 +287,7 @@
 
     def x_step(k):
         def one(o, side):
-            x_copy(o, nbr_x, 0, 2, nbr_y).wait_recv()
+            x_copy(o, nbr_x, 0, 0, nbr_y).wait_recv()
             x_copy(o, nbr_x, 0, 2, nbr_y).start()
 
         if square:
@@ -294,7 +296,7 @@
 
     def y_step(k):
         def one(o, side):
-            x_copy(o, nbr_y, 1, 2, nbr_x).wait_recv()
+            x_copy(o, nbr_y, 1, 1, nbr_x).wait_recv()
             x_copy(o, nbr_y, 1, 2, nbr_x).start()
 
         if square:
@@ -307,26 +309,30 @@
 
     def dp_copy(o):
         ref = down_x.at[2 * o + core]
-        return remote(ref, ref, dp_send.at[o], dp_recv.at[o], s, partner)
+        return remote(ref, ref, dp_send.at[0], dp_recv.at[o], s, partner)
 
     def dp_wait(o):
         ref = down_x.at[2 * o + 1 - core]
-        remote(ref, ref, dp_send.at[o], dp_recv.at[o], s, partner).wait_recv()
-
-    def d_start():
-        dx_copy.wait_recv()
-
-        @pl.when(has_up)
+        remote(ref, ref, dp_send.at[0], dp_recv.at[o], s, partner).wait_recv()
+
+    def at_edge(o):
+        return (o == 0) | (o == Z - 1)
+
+    def d_start(edges):
+        if edges:
+            dx_copy.wait_recv()
+            dp_copy(z).start()
+        mine = at_edge(z) if edges else jnp.logical_not(at_edge(z))
+
+        @pl.when(mine & has_up)
         def _():
             zd_copy(z, 0, z + 1).start()
 
-        @pl.when(has_down)
+        @pl.when(mine & has_down)
         def _():
             zd_copy(z, 1, z - 1).start()
 
-        dp_copy(z).start()
-
-    def d_step(k):
+    def d_step(k, edges=None):
         def one(o, side):
             zd_copy(o, side, z).wait_recv()
 
@@ -336,8 +342,13 @@
 
             dp_copy(o).start()
 
+        def some(o, side):
+            pl.when(at_edge(o) if edges else jnp.logical_not(at_edge(o)))(
+                functools.partial(one, o, side)
+            )
+
         with jax.named_scope(f"d{k}"):
-            each_slice(k, one)
+            each_slice(k, one if edges is None else some)
 
     def finish_row(k, parts):
         def one(o, side):
@@ -345,7 +356,7 @@
                 p = order[i]
                 if i > 0 and square:
                     for h in ((1,), (0,), (0, 1))[i - 1]:
-                        x_copy(o, p, h, 0, p).wait_recv()
+                        x_copy(o, p, h, i - 1, p).wait_recv()
                 elif i > 0:
                     for h in range(H):
                         x_copy(o, p, h, i - 1, p).wait_recv()
@@ -415,7 +426,7 @@
 
     def conv_copy(to):
         return remote(
-            conv_out.at[to], conv_in.at[t], a2a_send.at[to], a2a_recv.at[t], s, to
+            conv_out.at[to], conv_in.at[t], a2a_send.at[0], a2a_recv.at[t], s, to
         )
 
     def conv_flush(inner):
@@ -430,14 +441,19 @@
                     for c in range(2):
                         conv_copy(2 * to + c).start()
 
-    marks = [1 + (T - 1) * i // 7 for i in (3, 5, 7)]
+    marks = [1 + (T - 2) * i // 6 for i in (1, 2, 4, 6)]
     conv_some(1, marks[0])
+    for i in range(1, S):
+        own_w[i].wait()
+        p_copy(z, order[i]).start()
+    conv_some(marks[0], marks[1])
     z_step(1, 0)
-    conv_some(marks[0], marks[1])
+    conv_some(marks[1], marks[2])
     z_step(1, 1)
-    conv_some(marks[1], marks[2])
+    conv_some(marks[2], marks[3])
     z_step(2, 0)
     conv_flush(True)
+    conv_some(marks[3], T)
     with jax.named_scope("rimwait"):
         rim_copy.wait()
     same = (rim_in[HALO : HALO + 1, :].astype(F32) == ids_row_ref[0:1, 0:1].astype(F32)) & (s > 0)
@@ -446,6 +462,8 @@
     x_step(1)
     z_step(2, 1)
     conv_flush(False)
+    if paired:
+        d_start(True)
     y_step(1)
     conv_in[t, :, :] = conv_out[t, :, :]
 
@@ -491,6 +509,34 @@
     for e in range(E):
         picks[e, :, :] = (slot_r[e : e + 1, :] == cap_i).astype(F32).astype(BF16)
 
+    def piece_cols(j):
+        return pl.ds(pl.multiple_of(j * piece, piece), piece)
+
+    def finish_last():
+        for k in (Z - 2, Z - 1):
+            finish_row(k, all_parts[-1:])
+
+    def column(array, expert):
+        mine = lane[:, : array.shape[1]] == expert
+        return jnp.sum(jnp.where(mine, array, jnp.float32(0.0)), axis=1, keepdims=True)
+
+    zero = jnp.float32(0.0)
+    slot_iota = lax.broadcasted_iota(jnp.int32, (rows, cap), 1).astype(F32)
+    ff = gate_w.shape[2]
+    ff_step = min(ff, 256)
+
+
+    if paired:
+        for c in loads[8:]:
+            c.wait()
+        blank = jnp.zeros((router_all.shape[0] - G - E, D), F32)
+        router_all[...] = jnp.concatenate(
+            [group_router_ref[...].astype(F32), expert_router_ref[...].astype(F32), blank], axis=0
+        ).astype(BF16)
+        for e, at in enumerate((s, nbr_y)):
+            spread_all[e, :, :] = jnp.where(
+                column(slot, at) == slot_iota, jnp.float32(1.0), zero
+            ).astype(BF16)
     all_parts = tuple(range(S))
     for k in range(3, Z):
         z_step(k, 0)
@@ -511,7 +557,7 @@
             remote(
                 conv_out.at[source],
                 conv_in.at[source],
-                a2a_send.at[source],
+                a2a_send.at[0],
                 a2a_recv.at[source],
                 s,
                 source,
@@ -519,7 +565,8 @@
             total = total + jnp.sum(conv_in[source].astype(F32), axis=1, keepdims=True)
     if paired:
         with jax.named_scope("d0"):
-            d_start()
+            d_start(False)
+            d_step(1, True)
     with jax.named_scope("act"):
         average = total / (T * width)
         total = jnp.zeros((rows, 1), F32)
@@ -540,23 +587,6 @@
     prompt = others[:2] if square else others
     late = others[2:] if square else []
 
-    def piece_cols(j):
-        return pl.ds(pl.multiple_of(j * piece, piece), piece)
-
-    def finish_last():
-        for k in (Z - 2, Z - 1):
-            finish_row(k, all_parts[-1:])
-
-    def column(array, expert):
-        mine = lane[:, : array.shape[1]] == expert
-        return jnp.sum(jnp.where(mine, array, jnp.float32(0.0)), axis=1, keepdims=True)
-
-    zero = jnp.float32(0.0)
-    slot_iota = lax.broadcasted_iota(jnp.int32, (rows, cap), 1).astype(F32)
-    ff = gate_w.shape[2]
-    ff_step = min(ff, 256)
-
-
     if paired:
         C = CHUNKS
         part = cap // C
@@ -567,15 +597,15 @@
 
         def a_copy(j):
             return remote(
-                outgoing.at[0, j], arrived.at[0, j], ex_send.at[0, j], ex_recv.at[0, j], nbr_x, t
+                outgoing.at[0, j], arrived.at[0, j], ex_send.at[0], ex_recv.at[0], nbr_x, t
             )
 
         def b_copy(j, c):
             return remote(
                 outgoing.at[1, j, chunk(c), :],
                 arrived.at[1, j, chunk(c), :],
-                ex_send.at[1 + c, j],
-                ex_recv.at[1 + c, j],
+                ex_send.at[0],
+                ex_recv.at[1 + c * S + j],
                 nbr_y,
                 t,
             )
@@ -584,8 +614,8 @@
             return remote(
                 arrived.at[1, j, chunk(c), :],
                 arrived.at[2, j, chunk(c), :],
-                ex_send.at[1 + C + c, j],
-                ex_recv.at[1 + C + c, j],
+                ex_send.at[0],
+                ex_recv.at[1 + C * S + c],
                 nbr_x,
                 t,
             )
@@ -598,7 +628,7 @@
             return remote(
                 h_out.at[kind, at, :],
                 h_in.at[kind, at, :],
-                hx_send.at[kind, c],
+                hx_send.at[0],
                 hx_recv.at[kind, c],
                 nbr_x,
                 t,
@@ -607,19 +637,30 @@
         def rt_copy(q, c):
             return remote(
                 back_out.at[q, chunk(c), :],
-                back_in.at[q, chunk(c), :],
-                rt_send.at[q, c],
-                rt_recv.at[q, c],
+                back_in.at[q, pl.ds(cap + c * part, part), :],
+                rt_send.at[0],
+                rt_recv.at[q],
                 nbr_y,
                 t,
             )
 
+        def a_wait():
+            ref = arrived.at[0]
+            remote(ref, ref, ex_send.at[0], ex_recv.at[0], nbr_x, t).wait_recv()
+
+        def f_wait(c):
+            ref = arrived.at[2, :, chunk(c), :]
+            remote(ref, ref, ex_send.at[0], ex_recv.at[1 + C * S + c], nbr_x, t).wait_recv()
+
+        def rt_wait(q):
+            ref = back_in.at[q, pl.ds(cap, cap), :]
+            remote(ref, ref, rt_send.at[0], rt_recv.at[q], nbr_y, t).wait_recv()
+
         y_order = [nbr_y, diag, s, nbr_x]
 
         def project(i, j):
             with jax.named_scope("wpwait"):
-                for o in range(Z):
-                    p_wait(o, j)
+                p_wait(j)
             cols = piece_cols(j)
             acc = residual[:, cols].astype(F32)
             acc = acc + jnp.dot(act[...], wfull[j], preferred_element_type=F32)
@@ -629,6 +670,9 @@
                 picks[nbr_y], state, preferred_element_type=F32
             ).astype(BF16)
             b_copy(j, 0).start()
+            if i == 0:
+                for c in range(1, C):
+                    b_copy(j, c).start()
             outgoing[0, j, :, :] = jnp.dot(
                 picks[s], state, preferred_element_type=F32
             ).astype(BF16)
@@ -648,20 +692,15 @@
         mate_lane = (router_lane == s + G) | (router_lane == nbr_x + G)
 
         def gate_up(source, at, count, target):
-            def square_step(j, squares):
+            total = jnp.zeros((count, 1), F32)
+            for j in range(S):
                 x = source[j, at, :].astype(F32)
-                return squares + jnp.sum(x * x, axis=1, keepdims=True)
-
-            total = lax.fori_loop(0, S, square_step, jnp.zeros((count, 1), F32))
+                total = total + jnp.sum(x * x, axis=1, keepdims=True)
             row_scale = lax.rsqrt(total / D + epsilon)
-
-            def norm_step(j, _):
-                cols = piece_cols(j)
+            for j in range(S):
+                cols = slice(j * piece, (j + 1) * piece)
                 x = source[j, at, :].astype(F32)
                 normed_in[0:count, cols] = (x * row_scale * gain_moe_ref[:, cols]).astype(BF16)
-                return 0
-
-            lax.fori_loop(0, S, norm_step, 0)
             logits = lax.dot_general(
                 normed_in[0:count, :],
                 router_all[...],
@@ -675,23 +714,17 @@
 
             weight = over(own_group_lane) / over(group_lane) * over(own_lane) / over(mate_lane)
 
-            def up_step(j, _):
-                cols = pl.ds(pl.multiple_of(j * ff_step, ff_step), ff_step)
+            for j in range(ff // ff_step):
+                cols = slice(j * ff_step, (j + 1) * ff_step)
                 x = normed_in[0:count, :]
                 g = jnp.dot(x, gate_w[0, :, cols], preferred_element_type=F32)
                 u = jnp.dot(x, up_w[0, :, cols], preferred_element_type=F32)
                 target[at, cols] = (g / (1.0 + jnp.exp(-g)) * u * weight).astype(BF16)
-                return 0
-
-            lax.fori_loop(0, ff // ff_step, up_step, 0)
 
         def each_block(k, act_on):
             def pair(o, side):
-                def one(c2, _):
+                for c2 in range(2):
                     act_on(2 * o + c2)
-                    return 0
-
-                lax.fori_loop(0, 2, one, 0)
 
             if k == 0:
                 pair(z, 0)
@@ -721,51 +754,40 @@
                         each_slice(k, lambda o, side: dp_wait(o))
                 each_block(k, block_of)
 
+        everyone = pl.ds(0, cap)
         for i, j in enumerate(order):
             with jax.named_scope(f"project{i}"):
                 project(i, j)
             if i == 0:
                 finish_last()
+            if i == 2:
+                forward(0, 0, 1)
         for c in range(1, C):
-            for j in order:
+            for j in order[1:]:
                 b_copy(j, c).start()
-        forward(0, 0, S // 2)
-        for c in loads[8:]:
-            c.wait()
-        blank = jnp.zeros((router_all.shape[0] - G - E, D), F32)
-        router_all[...] = jnp.concatenate(
-            [group_router_ref[...].astype(F32), expert_router_ref[...].astype(F32), blank], axis=0
-        ).astype(BF16)
-        forward(0, S // 2, S)
-        everyone = pl.ds(0, cap)
+        with jax.named_scope("guA"):
+            gate_up(outgoing.at[0], everyone, cap, h_own.at[0])
+        forward(0, 1, 3)
+        d_step(1, False)
+        forward(0, 3, 4)
         with jax.named_scope("guB0"):
             gate_up(arrived.at[1], chunk(0), part, h_own.at[1])
-        forward(1, 0, S // 2)
-        with jax.named_scope("guA"):
-            gate_up(outgoing.at[0], everyone, cap, h_own.at[0])
-        forward(1, S // 2, S)
-        d_step(1)
+        forward(1, 0, 4)
         with jax.named_scope("fw0"):
-            for j in y_order:
-                f_copy(j, 0).wait_recv()
+            f_wait(0)
         with jax.named_scope("guF0"):
             gate_up(arrived.at[2], chunk(0), part, h_out.at[1])
         hx_copy(1, 0).start()
         a_copy(order[2]).start()
         with jax.named_scope("guB1"):
             gate_up(arrived.at[1], chunk(1), part, h_own.at[1])
+        d_step(2)
         with jax.named_scope("fw1"):
-            for j in y_order:
-                f_copy(j, 1).wait_recv()
+            f_wait(1)
         with jax.named_scope("guF1"):
             gate_up(arrived.at[2], chunk(1), part, h_out.at[1])
         hx_copy(1, 1).start()
         a_copy(order[3]).start()
-        d_step(2)
-        for e, at in enumerate((s, nbr_y)):
-            spreads[e, :, :] = jnp.where(
-                column(slot, at) == slot_iota, jnp.float32(1.0), zero
-            ).astype(BF16)
         with jax.named_scope("hw0"):
             hx_copy(1, 0).wait_recv()
         down_b(0, 0)
@@ -775,44 +797,56 @@
         down_b(0, 1)
         down_b(1, 1)
         with jax.named_scope("aw"):
-            for j in order:
-                a_copy(j).wait_recv()
+            a_wait()
         with jax.named_scope("guX"):
             gate_up(arrived.at[0], everyone, cap, h_out.at[0])
         hx_copy(0, 0).start()
+        for k in range(3, Z):
+            d_step(k)
         for k in range(2, Z):
-            if k > 2:
-                d_step(k)
             for c in range(C):
                 down_b(k, c)
+        with jax.named_scope("own_down"):
+            for q in range(T):
+                own_down[q, :, :] = jnp.dot(
+                    h_own[0], down_w[0, :, q * wide : (q + 1) * wide], preferred_element_type=F32
+                )
+
+        def combine_b(q):
+            rt_wait(q)
+            mixed = jnp.dot(
+                spread_all[1], back_in[q, cap : 2 * cap, :], preferred_element_type=F32
+            )
+            base_out[q, :, :] = hidden[:, wide_cols(q)].astype(F32) + mixed
+
+        def combine_a(q):
+            acc = own_down[q] + jnp.dot(h_in[0], down_x[q], preferred_element_type=F32)
+            mixed = jnp.dot(spread_all[0], acc.astype(BF16), preferred_element_type=F32)
+            out_ref[:, wide_cols(q)] = (base_out[q] + mixed).astype(BF16)
+
+        def combine(q):
+            combine_b(q)
+            combine_a(q)
+
+        ahead = min(2, Z)
+        for k in range(ahead):
+            with jax.named_scope(f"comb_b{k}"):
+                each_block(k, combine_b)
         with jax.named_scope("hwA"):
             hx_copy(0, 0).wait_recv()
 
-        def combine(q):
-            for c in range(C):
-                rt_copy(q, c).wait_recv()
-            cols = wide_cols(q)
-            acc = hidden[:, cols].astype(F32)
-            acc = acc + jnp.dot(spreads[0], both(0, everyone, q), preferred_element_type=F32)
-            acc = acc + jnp.dot(spreads[1], back_in[q], preferred_element_type=F32)
-            out_ref[:, cols] = acc.astype(BF16)
-
         for k in range(Z):
             with jax.named_scope(f"combine{k}"):
-                each_block(k, combine)
+                each_block(k, combine_a if k < ahead else combine)
 
         with jax.named_scope("sendwait"):
             dx_copy.wait_send()
-            for i in range(S):
-                a_copy(i).wait_send()
-                for c in range(C):
-                    b_copy(i, c).wait_send()
-                    f_copy(i, c).wait_send()
-            hx_copy(0, 0).wait_send()
-            for c in range(C):
-                hx_copy(1, c).wait_send()
-                for q in range(T):
-                    rt_copy(q, c).wait_send()
+            sets = outgoing.at[0:3]
+            remote(sets, sets, ex_send.at[0], ex_recv.at[0], nbr_x, t).wait_send()
+            remote(h_out, h_out, hx_send.at[0], hx_recv.at[0, 0], nbr_x, t).wait_send()
+            remote(back_out, back_out, rt_send.at[0], rt_recv.at[0], nbr_y, t).wait_send()
+            ref = down_x.at[0:Z]
+            remote(ref, ref, dp_send.at[0], dp_recv.at[0], s, partner).wait_send()
 
             @pl.when(has_up)
             def _():
@@ -821,15 +855,11 @@
             @pl.when(has_down)
             def _():
                 zd_copy(z, 1, z - 1).wait_send()
-
-            dp_copy(z).wait_send()
 
             def d_sent(o, side):
                 @pl.when(has_down if side else has_up)
                 def _():
                     zd_copy(o, side, z - 1 if side else z + 1).wait_send()
-
-                dp_copy(o).wait_send()
 
             for k in range(1, Z):
                 each_slice(k, d_sent)
@@ -877,8 +907,7 @@
 
         def project(j, squares):
             with jax.named_scope("wpwait"):
-                for o in range(Z):
-                    p_wait(o, j)
+                p_wait(j)
             cols = piece_cols(j)
             acc = residual[:, cols].astype(F32)
             part = jnp.dot(act[...], wfull[j], preferred_element_type=F32)
@@ -1013,25 +1042,21 @@
             def _():
                 z_copy(z, h, 1, z - 1).wait_send()
 
-        for j in range(S):
-            p_copy(z, j).wait_send()
         def sent(o, side):
-            beyond = has_down if side else has_up
             for h in range(H):
 
-                @pl.when(beyond)
+                @pl.when(has_down if side else has_up)
                 def _():
                     z_copy(o, h, side, z - 1 if side else z + 1).wait_send()
 
-                for j in range(3 if square else S - 1):
-                    x_copy(o, s, h, j, lax.rem(s + 1, S)).wait_send()
-            for j in range(S):
-                p_copy(o, j).wait_send()
-
         for k in range(1, Z):
             each_slice(k, sent)
-        for k in range(1, T):
-            conv_copy(lax.rem(t + k, T)).wait_send()
+        ref = wfull.at[0 : S - 1, pl.ds(0, (Z - 1) * wrows), :]
+        remote(ref, ref, wx_send.at[0], wx_recv.at[0, 0, 0], order[1], t).wait_send()
+        ref = wfull.at[:, pl.ds(0, Z * wrows), :]
+        remote(ref, ref, wp_send.at[0], wp_recv.at[0], s, partner).wait_send()
+        ref = conv_out.at[0 : T - 1]
+        remote(ref, ref, a2a_send.at[0], a2a_recv.at[0], s, partner).wait_send()
 
 
 def body(
@@ -1064,6 +1089,7 @@
     dma = pltpu.SemaphoreType.DMA
     piece = D // S
     Z = T // 2
+    paired = S == 4 and E == S and E == 2 * G
     return pl.pallas_call(
         functools.partial(kernel, S, T, G),
         out_shape=pltpu.VMEM((rows, D), BF16),
@@ -1110,31 +1136,34 @@
             pltpu.VMEM((2, cap, ff), BF16),
             pltpu.VMEM((2, cap, ff), BF16),
             pltpu.VMEM((T, cap, D // T), BF16),
-            pltpu.VMEM((T, cap, D // T), BF16),
+            pltpu.VMEM((T, 2 * cap, D // T), BF16),
+            pltpu.VMEM((T, cap, D // T), F32),
+            pltpu.VMEM((2, rows, cap), BF16),
+            pltpu.VMEM((T, rows, D // T), F32),
             dma((15,)),
             dma((S,)),
             dma((2,)),
             dma((2, Z, 2)),
             dma((Z, 2)),
-            dma((max(S - 1, 3), Z, 2)),
-            dma((S, Z, 2)),
-            dma((Z, S)),
-            dma((Z, S)),
+            dma((1,)),
+            dma((S - 1, Z, 2)),
+            dma((1,)),
+            dma((S,)),
+            dma((1,)),
             dma((T,)),
+            dma((1, 1) if paired else (S, S)),
+            dma((1, 1) if paired else (S, S)),
+            dma((1, 1) if paired else (S, S)),
+            dma((1, 1) if paired else (S, S)),
+            dma((1,)),
+            dma((1 + CHUNKS * (S + 1),)),
+            dma((1,)),
+            dma((2, CHUNKS)),
+            dma((1,)),
             dma((T,)),
-            dma((S, S)),
-            dma((S, S)),
-            dma((S, S)),
-            dma((S, S)),
-            dma((1 + 2 * CHUNKS, S)),
-            dma((1 + 2 * CHUNKS, S)),
-            dma((2, CHUNKS)),
-            dma((2, CHUNKS)),
-            dma((T, CHUNKS)),
-            dma((T, CHUNKS)),
             dma((2, Z)),
             dma((Z,)),
-            dma((Z,)),
+            dma((1,)),
             dma((Z,)),
             dma((2,)),
         ],

time: 75 us -> 71.2 us (0.949)
  Pallas kernels: 72.6 us -> 68.8 us
    pallas_call x1, Pallas kernels: 72.6 us -> 68.8 us  [body(): pl.pallas_call(functools.partial(kernel, S, T, G), out_shape=pltpu.VMEM((...]
where the time goes in v5:
time: 71.2 us; the launch traced here: 71 us
  Pallas kernels  68.8 us (97%)
  local copies, waits for them, and re-layouts  2.18 us (3%)
    pallas_call x1, Pallas kernels, body(): pl.pallas_call(functools.partial(kernel, S, T, G), out_shape=pltpu.VMEM((...  68.8 us

profile of v5, /device:TPU:0, one launch (start us, length us, event | category | flops | bytes accessed | tf_op | source)
XLA Modules:
  0.0 71.0 jit_solution(5658122581004430644)
XLA Ops:
  0.0 1.3 %broadcast_in_dim.12.ids_hbm = s32[1,1536]{1,0:T(1,128)} reshape(s32[1536]{0:T(1024)} %param.17) | data formatting | bytes 12288 | tf_op jit(solution)/shard_map/broadcast_in_dim | solution.py:1176
  1.3 68.8 %shard_map.145 = bf16[192,2048]{1,0:T(8,128)(2,1)S(1)} custom-call(bf16[1536,256]{1,0:T(8,128)(2,1)} %value_hbm.1, bf16[1536,256]{1,0:T(8,128)(2,1)} %gate_hbm.1, s32[1,1536]{1,0:T(1,128)} %broadcast_in_dim.12.ids_hbm, bf16[31,256]{1,0:T(8,128)(2,1)} %kernel_hbm.1, f32[1,2048]{1,0:T(1,128)} %bitcast.7, f32[1,2048]{1,0:T(1,128)} %bitcast.8, ...), custom_call_target="tpu_custom_call" | custom-call | tf_op jit(solution)/shard_map/pallas_call | solution.py:1093
  70.1 0.9 %copy.17 = bf16[192,2048]{1,0:T(8,128)(2,1)} copy(bf16[192,2048]{1,0:T(8,128)(2,1)S(1)} %shard_map.145) | data formatting | bytes 1572864

commit v6 on v5

--- a/solution.py
+++ b/solution.py
@@ -80,7 +80,7 @@
     h_in,
     back_out,
     back_in,
-    own_down,
+    h_rows,
     spread_all,
     base_out,
     local_sem,
@@ -195,6 +195,161 @@
     for c in loads[1:4]:
         c.start()
 
+    with jax.named_scope("barrier"):
+        pl.semaphore_wait(barrier, T + S - 2)
+
+    def w_ref(o, p, h):
+        base = pl.multiple_of((2 * o + core) * wrows + h * part_rows, part_rows)
+        return wfull.at[p, pl.ds(base, part_rows), :]
+
+    def z_copy(o, h, up, to):
+        ref = w_ref(o, s, h)
+        return remote(ref, ref, wz_send.at[up], wz_recv.at[o, h], s, 2 * to + core)
+
+    def x_copy(o, p, h, role, to):
+        ref = w_ref(o, p, h)
+        return remote(ref, ref, wx_send.at[0], wx_recv.at[role, o, h], to, t)
+
+    def p_copy(o, p):
+        rows_at = pl.ds(pl.multiple_of((2 * o + core) * wrows, wrows), wrows)
+        ref = wfull.at[p, rows_at, :]
+        return remote(ref, ref, wp_send.at[0], wp_recv.at[p], s, partner)
+
+    def p_wait(p):
+        ref = wfull.at[p, pl.ds(0, Z * wrows), :]
+        remote(ref, ref, wp_send.at[0], wp_recv.at[p], s, partner).wait_recv()
+
+    has_up = z + 1 < Z
+    has_down = z > 0
+    own_w[0].wait()
+    for h in range(H):
+
+        @pl.when(has_up)
+        def _():
+            z_copy(z, h, 0, z + 1).start()
+
+        @pl.when(has_down)
+        def _():
+            z_copy(z, h, 1, z - 1).start()
+
+    for c in own_w[1:]:
+        c.start()
+    for c in loads[4:]:
+        c.start()
+    dx_copy = remote(down_stage, down_x.at[t], dx_sem.at[0], dx_sem.at[1], nbr_x, t)
+    if paired:
+        stage.wait()
+        dx_copy.start()
+    p_copy(z, s).start()
+
+    def sides(k):
+        return ((z - k, z - k >= 0, 0), (z + k, z + k < Z, 1))
+
+    def each_slice(k, act_on):
+        for o, there, side in sides(k):
+            pl.when(there)(functools.partial(act_on, o, side))
+
+    def z_step(k, h):
+        def one(o, side):
+            z_copy(o, h, side, z).wait_recv()
+            beyond = has_down if side else has_up
+
+            @pl.when(beyond)
+            def _():
+                z_copy(o, h, side, z - 1 if side else z + 1).start()
+
+            if square:
+                x_copy(o, s, h, 0, nbr_x).start()
+                x_copy(o, s, h, 1, nbr_y).start()
+            else:
+                for j in range(1, S):
+                    x_copy(o, s, h, j - 1, lax.rem(s + j, S)).start()
+            if h == H - 1:
+                p_copy(o, s).start()
+
+        with jax.named_scope(f"z{k}{h}"):
+            each_slice(k, one)
+
+    def x_step(k):
+        def one(o, side):
+            x_copy(o, nbr_x, 0, 0, nbr_y).wait_recv()
+            x_copy(o, nbr_x, 0, 2, nbr_y).start()
+
+        if square:
+            with jax.named_scope(f"x{k}"):
+                each_slice(k, one)
+
+    def y_step(k):
+        def one(o, side):
+            x_copy(o, nbr_y, 1, 1, nbr_x).wait_recv()
+            x_copy(o, nbr_y, 1, 2, nbr_x).start()
+
+        if square:
+            with jax.named_scope(f"y{k}"):
+                each_slice(k, one)
+
+    def zd_copy(o, side, to):
+        ref = down_x.at[2 * o + core]
+        return remote(ref, ref, zd_send.at[side], zd_recv.at[o], s, 2 * to + core)
+
+    def dp_copy(o):
+        ref = down_x.at[2 * o + core]
+        return remote(ref, ref, dp_send.at[0], dp_recv.at[o], s, partner)
+
+    def dp_wait(o):
+        ref = down_x.at[2 * o + 1 - core]
+        remote(ref, ref, dp_send.at[0], dp_recv.at[o], s, partner).wait_recv()
+
+    def at_edge(o):
+        return (o == 0) | (o == Z - 1)
+
+    def d_start(edges):
+        if edges:
+            dx_copy.wait_recv()
+            dp_copy(z).start()
+        mine = at_edge(z) if edges else jnp.logical_not(at_edge(z))
+
+        @pl.when(mine & has_up)
+        def _():
+            zd_copy(z, 0, z + 1).start()
+
+        @pl.when(mine & has_down)
+        def _():
+            zd_copy(z, 1, z - 1).start()
+
+    def d_step(k, edges=None):
+        def one(o, side):
+            zd_copy(o, side, z).wait_recv()
+
+            @pl.when(has_down if side else has_up)
+            def _():
+                zd_copy(o, side, z - 1 if side else z + 1).start()
+
+            dp_copy(o).start()
+
+        def some(o, side):
+            pl.when(at_edge(o) if edges else jnp.logical_not(at_edge(o)))(
+                functools.partial(one, o, side)
+            )
+
+        with jax.named_scope(f"d{k}"):
+            each_slice(k, one if edges is None else some)
+
+    def finish_row(k, parts):
+        def one(o, side):
+            for i in parts:
+                p = order[i]
+                if square:
+                    for h in ((1,), (0,), (0, 1))[i - 1]:
+                        x_copy(o, p, h, i - 1, p).wait_recv()
+                else:
+                    for h in range(H):
+                        x_copy(o, p, h, i - 1, p).wait_recv()
+                p_copy(o, p).start()
+
+        with jax.named_scope(f"fin{k}{parts[0]}"):
+            each_slice(k, one)
+
     loads[0].wait()
     ids_row = jnp.broadcast_to(ids_row_ref[...], (8, tokens))
     position = lax.broadcasted_iota(jnp.int32, (8, tokens), 1)
@@ -211,159 +366,6 @@
     for c in range(tokens // lanes):
         across = jnp.broadcast_to(least_row[0:1, c * lanes : (c + 1) * lanes], (lanes, lanes))
         least_tap[c * lanes : (c + 1) * lanes, :] = across.T
-
-    with jax.named_scope("barrier"):
-        pl.semaphore_wait(barrier, T + S - 2)
-
-    def w_ref(o, p, h):
-        base = pl.multiple_of((2 * o + core) * wrows + h * part_rows, part_rows)
-        return wfull.at[p, pl.ds(base, part_rows), :]
-
-    def z_copy(o, h, up, to):
-        ref = w_ref(o, s, h)
-        return remote(ref, ref, wz_send.at[up, o, h], wz_recv.at[o, h], s, 2 * to + core)
-
-    def x_copy(o, p, h, role, to):
-        ref = w_ref(o, p, h)
-        return remote(ref, ref, wx_send.at[0], wx_recv.at[role, o, h], to, t)
-
-    def p_copy(o, p):
-        rows_at = pl.ds(pl.multiple_of((2 * o + core) * wrows, wrows), wrows)
-        ref = wfull.at[p, rows_at, :]
-        return remote(ref, ref, wp_send.at[0], wp_recv.at[p], s, partner)
-
-    def p_wait(p):
-        ref = wfull.at[p, pl.ds(0, Z * wrows), :]
-        remote(ref, ref, wp_send.at[0], wp_recv.at[p], s, partner).wait_recv()
-
-    has_up = z + 1 < Z
-    has_down = z > 0
-    own_w[0].wait()
-    for h in range(H):
-
-        @pl.when(has_up)
-        def _():
-            z_copy(z, h, 0, z + 1).start()
-
-        @pl.when(has_down)
-        def _():
-            z_copy(z, h, 1, z - 1).start()
-
-    for c in own_w[1:]:
-        c.start()
-    for c in loads[4:]:
-        c.start()
-    dx_copy = remote(down_stage, down_x.at[t], dx_sem.at[0], dx_sem.at[1], nbr_x, t)
-    if paired:
-        stage.wait()
-        dx_copy.start()
-    p_copy(z, s).start()
-
-    def sides(k):
-        return ((z - k, z - k >= 0, 0), (z + k, z + k < Z, 1))
-
-    def each_slice(k, act_on):
-        for o, there, side in sides(k):
-            pl.when(there)(functools.partial(act_on, o, side))
-
-    def z_step(k, h):
-        def one(o, side):
-            z_copy(o, h, side, z).wait_recv()
-            beyond = has_down if side else has_up
-
-            @pl.when(beyond)
-            def _():
-                z_copy(o, h, side, z - 1 if side else z + 1).start()
-
-            if square:
-                x_copy(o, s, h, 0, nbr_x).start()
-                x_copy(o, s, h, 1, nbr_y).start()
-            else:
-                for j in range(1, S):
-                    x_copy(o, s, h, j - 1, lax.rem(s + j, S)).start()
-
-        with jax.named_scope(f"z{k}{h}"):
-            each_slice(k, one)
-
-    def x_step(k):
-        def one(o, side):
-            x_copy(o, nbr_x, 0, 0, nbr_y).wait_recv()
-            x_copy(o, nbr_x, 0, 2, nbr_y).start()
-
-        if square:
-            with jax.named_scope(f"x{k}"):
-                each_slice(k, one)
-
-    def y_step(k):
-        def one(o, side):
-            x_copy(o, nbr_y, 1, 1, nbr_x).wait_recv()
-            x_copy(o, nbr_y, 1, 2, nbr_x).start()
-
-        if square:
-            with jax.named_scope(f"y{k}"):
-                each_slice(k, one)
-
-    def zd_copy(o, side, to):
-        ref = down_x.at[2 * o + core]
-        return remote(ref, ref, zd_send.at[side, o], zd_recv.at[o], s, 2 * to + core)
-
-    def dp_copy(o):
-        ref = down_x.at[2 * o + core]
-        return remote(ref, ref, dp_send.at[0], dp_recv.at[o], s, partner)
-
-    def dp_wait(o):
-        ref = down_x.at[2 * o + 1 - core]
-        remote(ref, ref, dp_send.at[0], dp_recv.at[o], s, partner).wait_recv()
-
-    def at_edge(o):
-        return (o == 0) | (o == Z - 1)
-
-    def d_start(edges):
-        if edges:
-            dx_copy.wait_recv()
-            dp_copy(z).start()
-        mine = at_edge(z) if edges else jnp.logical_not(at_edge(z))
-
-        @pl.when(mine & has_up)
-        def _():
-            zd_copy(z, 0, z + 1).start()
-
-        @pl.when(mine & has_down)
-        def _():
-            zd_copy(z, 1, z - 1).start()
-
-    def d_step(k, edges=None):
-        def one(o, side):
-            zd_copy(o, side, z).wait_recv()
-
-            @pl.when(has_down if side else has_up)
-            def _():
-                zd_copy(o, side, z - 1 if side else z + 1).start()
-
-            dp_copy(o).start()
-
-        def some(o, side):
-            pl.when(at_edge(o) if edges else jnp.logical_not(at_edge(o)))(
-                functools.partial(one, o, side)
-            )
-
-        with jax.named_scope(f"d{k}"):
-            each_slice(k, one if edges is None else some)
-
-    def finish_row(k, parts):
-        def one(o, side):
-            for i in parts:
-                p = order[i]
-                if i > 0 and square:
-                    for h in ((1,), (0,), (0, 1))[i - 1]:
-                        x_copy(o, p, h, i - 1, p).wait_recv()
-                elif i > 0:
-                    for h in range(H):
-                        x_copy(o, p, h, i - 1, p).wait_recv()
-                p_copy(o, p).start()
-
-        with jax.named_scope(f"fin{k}{parts[0]}"):
-            each_slice(k, one)
 
     for c in loads[1:4]:
         c.wait()
@@ -426,7 +428,7 @@
 
     def conv_copy(to):
         return remote(
-            conv_out.at[to], conv_in.at[t], a2a_send.at[0], a2a_recv.at[t], s, to
+            conv_out.at[to], conv_in.at[t], a2a_send.at[0], a2a_recv.at[0], s, to
         )
 
     def conv_flush(inner):
@@ -537,37 +539,29 @@
             spread_all[e, :, :] = jnp.where(
                 column(slot, at) == slot_iota, jnp.float32(1.0), zero
             ).astype(BF16)
-    all_parts = tuple(range(S))
+    all_parts = tuple(range(1, S))
     for k in range(3, Z):
         z_step(k, 0)
         x_step(k - 1)
         z_step(k, 1)
         finish_row(k - 2, all_parts)
         y_step(k - 1)
-    finish_row(Z - 1, all_parts[:1])
     finish_row(Z - 2, all_parts[:-1])
     x_step(Z - 1)
     y_step(Z - 1)
-    finish_row(Z - 1, all_parts[1:-1])
+    finish_row(Z - 1, all_parts[:-1])
 
     with jax.named_scope("a2await"):
-        total = jnp.sum(conv_in[t].astype(F32), axis=1, keepdims=True)
-        for k in range(1, T):
-            source = lax.rem(t + k, T)
-            remote(
-                conv_out.at[source],
-                conv_in.at[source],
-                a2a_send.at[0],
-                a2a_recv.at[source],
-                s,
-                source,
-            ).wait_recv()
-            total = total + jnp.sum(conv_in[source].astype(F32), axis=1, keepdims=True)
+        ref = conv_in.at[0 : T - 1]
+        remote(ref, ref, a2a_send.at[0], a2a_recv.at[0], s, partner).wait_recv()
     if paired:
         with jax.named_scope("d0"):
             d_start(False)
             d_step(1, True)
     with jax.named_scope("act"):
+        total = jnp.zeros((rows, 1), F32)
+        for j in range(T):
+            total = total + jnp.sum(conv_in[j].astype(F32), axis=1, keepdims=True)
         average = total / (T * width)
         total = jnp.zeros((rows, 1), F32)
         for j in range(T):
@@ -595,9 +589,14 @@
         def chunk(c):
             return pl.ds(c * part, part)
 
-        def a_copy(j):
+        def a_copy(j, c):
             return remote(
-                outgoing.at[0, j], arrived.at[0, j], ex_send.at[0], ex_recv.at[0], nbr_x, t
+                outgoing.at[0, j, chunk(c), :],
+                arrived.at[0, j, chunk(c), :],
+                ex_send.at[0],
+                ex_recv.at[C * (S + 1) + c],
+                nbr_x,
+                t,
             )
 
         def b_copy(j, c):
@@ -605,7 +604,7 @@
                 outgoing.at[1, j, chunk(c), :],
                 arrived.at[1, j, chunk(c), :],
                 ex_send.at[0],
-                ex_recv.at[1 + c * S + j],
+                ex_recv.at[c * S + j],
                 nbr_y,
                 t,
             )
@@ -615,16 +614,13 @@
                 arrived.at[1, j, chunk(c), :],
                 arrived.at[2, j, chunk(c), :],
                 ex_send.at[0],
-                ex_recv.at[1 + C * S + c],
+                ex_recv.at[C * S + c],
                 nbr_x,
                 t,
             )
 
-        def h_rows(kind, c):
-            return pl.ds(0, cap) if kind == 0 else chunk(c)
-
         def hx_copy(kind, c):
-            at = h_rows(kind, c)
+            at = chunk(c)
             return remote(
                 h_out.at[kind, at, :],
                 h_in.at[kind, at, :],
@@ -637,23 +633,23 @@
         def rt_copy(q, c):
             return remote(
                 back_out.at[q, chunk(c), :],
-                back_in.at[q, pl.ds(cap + c * part, part), :],
+                back_in.at[q, chunk(c), :],
                 rt_send.at[0],
                 rt_recv.at[q],
                 nbr_y,
                 t,
             )
 
-        def a_wait():
-            ref = arrived.at[0]
-            remote(ref, ref, ex_send.at[0], ex_recv.at[0], nbr_x, t).wait_recv()
+        def a_wait(c):
+            ref = arrived.at[0, :, chunk(c), :]
+            remote(ref, ref, ex_send.at[0], ex_recv.at[C * (S + 1) + c], nbr_x, t).wait_recv()
 
         def f_wait(c):
             ref = arrived.at[2, :, chunk(c), :]
-            remote(ref, ref, ex_send.at[0], ex_recv.at[1 + C * S + c], nbr_x, t).wait_recv()
+            remote(ref, ref, ex_send.at[0], ex_recv.at[C * S + c], nbr_x, t).wait_recv()
 
         def rt_wait(q):
-            ref = back_in.at[q, pl.ds(cap, cap), :]
+            ref = back_in.at[q]
             remote(ref, ref, rt_send.at[0], rt_recv.at[q], nbr_y, t).wait_recv()
 
         y_order = [nbr_y, diag, s, nbr_x]
@@ -676,8 +672,7 @@
             outgoing[0, j, :, :] = jnp.dot(
                 picks[s], state, preferred_element_type=F32
             ).astype(BF16)
-            if i < 2:
-                a_copy(j).start()
+            a_copy(j, 0).start()
 
         def forward(c, first, last):
             with jax.named_scope(f"fwd{c}{first}"):
@@ -758,7 +753,7 @@
         for i, j in enumerate(order):
             with jax.named_scope(f"project{i}"):
                 project(i, j)
-            if i == 0:
+            if i == 1:
                 finish_last()
             if i == 2:
                 forward(0, 0, 1)
@@ -773,55 +768,67 @@
         with jax.named_scope("guB0"):
             gate_up(arrived.at[1], chunk(0), part, h_own.at[1])
         forward(1, 0, 4)
+        d_step(2, True)
         with jax.named_scope("fw0"):
             f_wait(0)
         with jax.named_scope("guF0"):
             gate_up(arrived.at[2], chunk(0), part, h_out.at[1])
         hx_copy(1, 0).start()
-        a_copy(order[2]).start()
+        a_copy(order[0], 1).start()
+        a_copy(order[1], 1).start()
         with jax.named_scope("guB1"):
             gate_up(arrived.at[1], chunk(1), part, h_own.at[1])
-        d_step(2)
+        with jax.named_scope("aw0"):
+            a_wait(0)
+        with jax.named_scope("guX0"):
+            gate_up(arrived.at[0], chunk(0), part, h_out.at[0])
         with jax.named_scope("fw1"):
             f_wait(1)
         with jax.named_scope("guF1"):
             gate_up(arrived.at[2], chunk(1), part, h_out.at[1])
         hx_copy(1, 1).start()
-        a_copy(order[3]).start()
+        a_copy(order[2], 1).start()
+        a_copy(order[3], 1).start()
+        hx_copy(0, 0).start()
+        d_step(2, False)
         with jax.named_scope("hw0"):
             hx_copy(1, 0).wait_recv()
         down_b(0, 0)
         down_b(1, 0)
+        down_b(2, 0)
+        with jax.named_scope("own_down"):
+            h_rows[0, :, :] = jnp.dot(
+                spread_all[0], h_own[0], preferred_element_type=F32
+            ).astype(BF16)
+            for q in range(T):
+                cols = slice(q * wide, (q + 1) * wide)
+                base_out[q, :, :] = hidden[:, cols].astype(F32) + jnp.dot(
+                    h_rows[0], down_w[0, :, cols], preferred_element_type=F32
+                )
         with jax.named_scope("hw1"):
             hx_copy(1, 1).wait_recv()
         down_b(0, 1)
         down_b(1, 1)
-        with jax.named_scope("aw"):
-            a_wait()
-        with jax.named_scope("guX"):
-            gate_up(arrived.at[0], everyone, cap, h_out.at[0])
-        hx_copy(0, 0).start()
         for k in range(3, Z):
             d_step(k)
-        for k in range(2, Z):
+        down_b(2, 1)
+        with jax.named_scope("aw1"):
+            a_wait(1)
+        with jax.named_scope("guX1"):
+            gate_up(arrived.at[0], chunk(1), part, h_out.at[0])
+        hx_copy(0, 1).start()
+        for k in range(3, Z):
             for c in range(C):
                 down_b(k, c)
-        with jax.named_scope("own_down"):
-            for q in range(T):
-                own_down[q, :, :] = jnp.dot(
-                    h_own[0], down_w[0, :, q * wide : (q + 1) * wide], preferred_element_type=F32
-                )
 
         def combine_b(q):
             rt_wait(q)
-            mixed = jnp.dot(
-                spread_all[1], back_in[q, cap : 2 * cap, :], preferred_element_type=F32
+            base_out[q, :, :] += jnp.dot(
+                spread_all[1], back_in[q], preferred_element_type=F32
             )
-            base_out[q, :, :] = hidden[:, wide_cols(q)].astype(F32) + mixed
 
         def combine_a(q):
-            acc = own_down[q] + jnp.dot(h_in[0], down_x[q], preferred_element_type=F32)
-            mixed = jnp.dot(spread_all[0], acc.astype(BF16), preferred_element_type=F32)
+            mixed = jnp.dot(h_rows[1], down_x[q], preferred_element_type=F32)
             out_ref[:, wide_cols(q)] = (base_out[q] + mixed).astype(BF16)
 
         def combine(q):
@@ -833,8 +840,11 @@
             with jax.named_scope(f"comb_b{k}"):
                 each_block(k, combine_b)
         with jax.named_scope("hwA"):
-            hx_copy(0, 0).wait_recv()
-
+            for c in range(C):
+                hx_copy(0, c).wait_recv()
+            h_rows[1, :, :] = jnp.dot(
+                spread_all[0], h_in[0], preferred_element_type=F32
+            ).astype(BF16)
         for k in range(Z):
             with jax.named_scope(f"combine{k}"):
                 each_block(k, combine_a if k < ahead else combine)
@@ -848,21 +858,16 @@
             ref = down_x.at[0:Z]
             remote(ref, ref, dp_send.at[0], dp_recv.at[0], s, partner).wait_send()
 
-            @pl.when(has_up)
-            def _():
-                zd_copy(z, 0, z + 1).wait_send()
-
-            @pl.when(has_down)
-            def _():
-                zd_copy(z, 1, z - 1).wait_send()
-
-            def d_sent(o, side):
-                @pl.when(has_down if side else has_up)
-                def _():
-                    zd_copy(o, side, z - 1 if side else z + 1).wait_send()
-
-            for k in range(1, Z):
-                each_slice(k, d_sent)
+            for zz in range(Z):
+                for side, count in ((0, zz + 1), (1, Z - zz)):
+                    if count < Z:
+                        ref = down_x.at[0:count]
+
+                        @pl.when(z == zz)
+                        def _():
+                            remote(
+                                ref, ref, zd_send.at[side], zd_recv.at[0], s, partner
+                            ).wait_send()
 
     else:
         def disp_copy(expert, j):
@@ -1032,25 +1037,17 @@
                 ret_copy(expert, j).wait_send()
 
     with jax.named_scope("sendwait"):
-        for h in range(H):
-
-            @pl.when(has_up)
-            def _():
-                z_copy(z, h, 0, z + 1).wait_send()
-
-            @pl.when(has_down)
-            def _():
-                z_copy(z, h, 1, z - 1).wait_send()
-
-        def sent(o, side):
-            for h in range(H):
-
-                @pl.when(has_down if side else has_up)
-                def _():
-                    z_copy(o, h, side, z - 1 if side else z + 1).wait_send()
-
-        for k in range(1, Z):
-            each_slice(k, sent)
+        for zz in range(Z):
+            for side, count in ((0, zz + 1), (1, Z - zz)):
+                if count < Z:
+                    ref = wfull.at[0, pl.ds(0, count * wrows), :]
+
+                    @pl.when(z == zz)
+                    def _():
+                        remote(
+                            ref, ref, wz_send.at[side], wz_recv.at[0, 0], s, partner
+                        ).wait_send()
+
         ref = wfull.at[0 : S - 1, pl.ds(0, (Z - 1) * wrows), :]
         remote(ref, ref, wx_send.at[0], wx_recv.at[0, 0, 0], order[1], t).wait_send()
         ref = wfull.at[:, pl.ds(0, Z * wrows), :]
@@ -1136,32 +1133,32 @@
             pltpu.VMEM((2, cap, ff), BF16),
             pltpu.VMEM((2, cap, ff), BF16),
             pltpu.VMEM((T, cap, D // T), BF16),
-            pltpu.VMEM((T, 2 * cap, D // T), BF16),
-            pltpu.VMEM((T, cap, D // T), F32),
+            pltpu.VMEM((T, cap, D // T), BF16),
+            pltpu.VMEM((2, rows, ff), BF16),
             pltpu.VMEM((2, rows, cap), BF16),
             pltpu.VMEM((T, rows, D // T), F32),
             dma((15,)),
             dma((S,)),
             dma((2,)),
-            dma((2, Z, 2)),
+            dma((2,)),
             dma((Z, 2)),
             dma((1,)),
             dma((S - 1, Z, 2)),
             dma((1,)),
             dma((S,)),
             dma((1,)),
-            dma((T,)),
+            dma((1,)),
             dma((1, 1) if paired else (S, S)),
             dma((1, 1) if paired else (S, S)),
             dma((1, 1) if paired else (S, S)),
             dma((1, 1) if paired else (S, S)),
             dma((1,)),
-            dma((1 + CHUNKS * (S + 1),)),
+            dma((CHUNKS * (S + 2),)),
             dma((1,)),
             dma((2, CHUNKS)),
             dma((1,)),
             dma((T,)),
-            dma((2, Z)),
+            dma((2,)),
             dma((Z,)),
             dma((1,)),
             dma((Z,)),

time: 71.2 us -> 69.5 us (0.976)
  Pallas kernels: 68.8 us -> 67.1 us
    pallas_call x1, Pallas kernels: 68.8 us -> 67.1 us  [body(): pl.pallas_call(functools.partial(kernel, S, T, G), out_shape=pltpu.VMEM((...]
where the time goes in v6:
time: 69.5 us; the launch traced here: 69.3 us
  Pallas kernels  67.1 us (97%)
  local copies, waits for them, and re-layouts  2.18 us (3%)
    pallas_call x1, Pallas kernels, body(): pl.pallas_call(functools.partial(kernel, S, T, G), out_shape=pltpu.VMEM((...  67.1 us

profile of v6, /device:TPU:0, one launch (start us, length us, event | category | flops | bytes accessed | tf_op | source)
XLA Modules:
  0.0 69.3 jit_solution(6799808983678088935)
XLA Ops:
  0.0 1.3 %broadcast_in_dim.12.ids_hbm = s32[1,1536]{1,0:T(1,128)} reshape(s32[1536]{0:T(1024)} %param.17) | data formatting | bytes 12288 | tf_op jit(solution)/shard_map/broadcast_in_dim | solution.py:1173
  1.3 67.1 %shard_map.145 = bf16[192,2048]{1,0:T(8,128)(2,1)S(1)} custom-call(bf16[1536,256]{1,0:T(8,128)(2,1)} %value_hbm.1, bf16[1536,256]{1,0:T(8,128)(2,1)} %gate_hbm.1, s32[1,1536]{1,0:T(1,128)} %broadcast_in_dim.12.ids_hbm, bf16[31,256]{1,0:T(8,128)(2,1)} %kernel_hbm.1, f32[1,2048]{1,0:T(1,128)} %bitcast.7, f32[1,2048]{1,0:T(1,128)} %bitcast.8, ...), custom_call_target="tpu_custom_call" | custom-call | tf_op jit(solution)/shard_map/pallas_call | solution.py:1090
  68.4 0.9 %copy.17 = bf16[192,2048]{1,0:T(8,128)(2,1)} copy(bf16[192,2048]{1,0:T(8,128)(2,1)S(1)} %shard_map.145) | data formatting | bytes 1572864

commit v7 on v6

--- a/solution.py
+++ b/solution.py
@@ -525,7 +525,7 @@
     zero = jnp.float32(0.0)
     slot_iota = lax.broadcasted_iota(jnp.int32, (rows, cap), 1).astype(F32)
     ff = gate_w.shape[2]
-    ff_step = min(ff, 256)
+    ff_step = min(ff, 512)
 
 
     if paired:
@@ -805,12 +805,12 @@
                 base_out[q, :, :] = hidden[:, cols].astype(F32) + jnp.dot(
                     h_rows[0], down_w[0, :, cols], preferred_element_type=F32
                 )
+        for k in range(3, Z):
+            d_step(k)
         with jax.named_scope("hw1"):
             hx_copy(1, 1).wait_recv()
         down_b(0, 1)
         down_b(1, 1)
-        for k in range(3, Z):
-            d_step(k)
         down_b(2, 1)
         with jax.named_scope("aw1"):
             a_wait(1)
@@ -835,7 +835,7 @@
             combine_b(q)
             combine_a(q)
 
-        ahead = min(2, Z)
+        ahead = min(3, Z)
         for k in range(ahead):
             with jax.named_scope(f"comb_b{k}"):
                 each_block(k, combine_b)

time: 69.5 us -> 69.2 us (level)
  no operation moved by 1% of the time
where the time goes in v7:
time: 69.2 us; the launch traced here: 69 us
  Pallas kernels  66.8 us (97%)
  local copies, waits for them, and re-layouts  2.18 us (3%)
    pallas_call x1, Pallas kernels, body(): pl.pallas_call(functools.partial(kernel, S, T, G), out_shape=pltpu.VMEM((...  66.8 us

profile of v7, /device:TPU:0, one launch (start us, length us, event | category | flops | bytes accessed | tf_op | source)
XLA Modules:
  0.0 69.0 jit_solution(798038544171457976)
XLA Ops:
  0.0 1.3 %broadcast_in_dim.12.ids_hbm = s32[1,1536]{1,0:T(1,128)} reshape(s32[1536]{0:T(1024)} %param.17) | data formatting | bytes 12288 | tf_op jit(solution)/shard_map/broadcast_in_dim | solution.py:1173
  1.3 66.8 %shard_map.145 = bf16[192,2048]{1,0:T(8,128)(2,1)S(1)} custom-call(bf16[1536,256]{1,0:T(8,128)(2,1)} %value_hbm.1, bf16[1536,256]{1,0:T(8,128)(2,1)} %gate_hbm.1, s32[1,1536]{1,0:T(1,128)} %broadcast_in_dim.12.ids_hbm, bf16[31,256]{1,0:T(8,128)(2,1)} %kernel_hbm.1, f32[1,2048]{1,0:T(1,128)} %bitcast.7, f32[1,2048]{1,0:T(1,128)} %bitcast.8, ...), custom_call_target="tpu_custom_call" | custom-call | tf_op jit(solution)/shard_map/pallas_call | solution.py:1090
  68.1 0.9 %copy.17 = bf16[192,2048]{1,0:T(8,128)(2,1)} copy(bf16[192,2048]{1,0:T(8,128)(2,1)S(1)} %shard_map.145) | data formatting | bytes 1572864
